TPU v7x, 32 devices: a whole 2x2x4 slice. The times are simulated.
32 devices in a mesh: sp: 8 (over z, x), tp: 4 (over y, core).
Axes of the slice: x: 2, y: 2, z: 4, core: 2. Of those that a mesh axis runs over, the one named last changes fastest.
Arguments:
- upstream: bfloat16 [2048, 2048], P('sp'), may hold values from -6 to 6
- stream: bfloat16 [2048, 2048], P('sp'), may hold values from -10 to 10
- routes: int32 [2048, 2], P('sp'), may hold values from 0 to 7, all different within a row; in each aligned block of 256 rows (0 to 255, 256 to 511, ...) at most 128 rows name the same one
- route_weights: float32 [2048, 2], P('sp'), may hold values from 0.1 to 1
- glu_value: bfloat16 [2048, 512], P('sp', 'tp'), may hold values from -6 to 6
- glu_gate: bfloat16 [2048, 512], P('sp', 'tp'), may hold values from -10 to 10
- conv_taps: float32 [31, 512], P(None, 'tp'), may hold values from -1 to 1
- conv_saved: bfloat16 [2048, 512], P('sp', 'tp'), may hold values from -600 to 600
- out_proj: bfloat16 [2048, 512], P(None, 'tp'), may hold values from -0.25 to 0.25
- expert_gate: bfloat16 [8, 2048, 2048], P('sp', None, 'tp'), may hold values from -0.125 to 0.125
- expert_up: bfloat16 [8, 2048, 2048], P('sp', None, 'tp'), may hold values from -0.125 to 0.125
- expert_down: bfloat16 [8, 2048, 2048], P('sp', 'tp'), may hold values from -0.125 to 0.125
Outputs:
- grad_stream: bfloat16 [2048, 2048], P('sp', 'tp')
- grad_value: bfloat16 [2048, 512], P('sp', 'tp')
- grad_gate: bfloat16 [2048, 512], P('sp', 'tp')
- grad_out_proj: float32 [2048, 512], P('sp', 'tp')
- grad_expert_gate: float32 [8, 2048, 2048], P('sp', None, 'tp')
- grad_expert_up: float32 [8, 2048, 2048], P('sp', None, 'tp')
- grad_expert_down: float32 [8, 2048, 2048], P('sp', 'tp')
Inputs may be any that keep to these rules, and one draw needn't show every extreme that they name: `routes`: each row names 2 different experts; among the 256 rows of one index of sp no expert is named more than 128 times, a bound that some block reaches.
All inputs are finite; a program needn't handle non-finite values.
Results may differ from a plain program's by a relative error of at most 0.014.
Values may be sent and summed in bfloat16 or wider, within the bound.
A program may use at most 128 MiB of HBM per device.

v0:
```python
import functools

import jax
import jax.numpy as jnp
from jax import lax
from jax.experimental import pallas as pl
from jax.experimental.pallas import tpu as pltpu
from jax.sharding import PartitionSpec as P


clamp_limit = 7.0
glu_alpha = 1.702
norm_eps = 1e-05


def contract_rows(left, right):
    return lax.dot_general(
        left, right, (((0,), (0,)), ((), ())), preferred_element_type=jnp.float32
    )


def times_transposed(left, right):
    return lax.dot_general(
        left, right, (((1,), (1,)), ((), ())), preferred_element_type=jnp.float32
    )


def pair_rows(block_routes, expert_count, capacity):
    tok_count, topk = block_routes.shape
    experts = jnp.arange(expert_count, dtype=jnp.int32)[None, :]
    hots = [(block_routes[:, k : k + 1] == experts).astype(jnp.float32) for k in range(topk)]
    before = (
        jnp.arange(tok_count)[:, None] > jnp.arange(tok_count)[None, :]
    ).astype(jnp.bfloat16)
    earlier = jnp.dot(before, sum(hots).astype(jnp.bfloat16), preferred_element_type=jnp.float32)
    slots = [jnp.sum(earlier * hot, axis=1).astype(jnp.int32) for hot in hots]
    return [block_routes[:, k] * capacity + slots[k] for k in range(topk)]


def select_pairs(targets, block_weights, row_count):
    rows = jnp.arange(row_count, dtype=jnp.int32)[:, None]
    hits = [target[None, :] == rows for target in targets]
    picks = sum(hit.astype(jnp.float32) for hit in hits).astype(jnp.bfloat16)
    row_weights = jnp.sum(
        sum(jnp.where(hit, block_weights[:, k][None, :], 0.0) for k, hit in enumerate(hits)), axis=1
    )
    return picks, row_weights


def greet(sp_count, tp_count):
    me, lane = lax.axis_index("sp"), lax.axis_index("tp")
    barrier = pltpu.get_barrier_semaphore()
    for step in range(1, sp_count):
        pl.semaphore_signal(
            barrier,
            inc=1,
            device_id={"sp": lax.rem(me + step, sp_count)},
            device_id_type=pl.DeviceIdType.MESH,
        )
    for step in range(1, tp_count):
        pl.semaphore_signal(
            barrier,
            inc=1,
            device_id={"tp": lax.rem(lane + step, tp_count)},
            device_id_type=pl.DeviceIdType.MESH,
        )
    pl.semaphore_wait(barrier, sp_count + tp_count - 2)


def remote(src, dst, send_sem, recv_sem, **target):
    return pltpu.make_async_remote_copy(
        src_ref=src,
        dst_ref=dst,
        send_sem=send_sem,
        recv_sem=recv_sem,
        device_id=target,
        device_id_type=pl.DeviceIdType.MESH,
    )


def dispatch_kernel(
    sp_count,
    tp_count,
    rows_ref,
    cot_ref,
    got_rows,
    got_cot,
    far_send,
    far_recv,
    side_send,
    side_recv,
    pair_send,
    pair_recv,
    own_sem,
):
    me, lane = lax.axis_index("sp"), lax.axis_index("tp")
    width = rows_ref.shape[2]
    chips = tp_count // 2
    partner = lane + 1 - 2 * lax.rem(lane, 2)
    sources, results = (rows_ref, cot_ref), (got_rows, got_cot)

    def place(which, block, column):
        return results[which].at[block, :, pl.ds(pl.multiple_of(column * width, width), width)]

    greet(sp_count, tp_count)

    def far(which, step):
        to = lax.rem(me + step, sp_count)
        return remote(
            sources[which].at[to],
            place(which, me, lane),
            far_send.at[which, step],
            far_recv.at[which, step],
            sp=to,
        )

    def beside(which, step, hop):
        block = lax.rem(me + sp_count - step, sp_count)
        source = sources[which].at[me] if step == 0 else place(which, block, lane)
        return remote(
            source,
            place(which, block, lane),
            side_send.at[which, step, hop],
            side_recv.at[which, step, hop],
            tp=lax.rem(lane + 2 * hop, tp_count),
        )

    def paired(which, step, hop):
        block = lax.rem(me + sp_count - step, sp_count)
        column = lax.rem(lane + tp_count - 2 * hop, tp_count)
        source = (
            sources[which].at[me] if step == 0 and hop == 0 else place(which, block, column)
        )
        return remote(
            source,
            place(which, block, column),
            pair_send.at[which, step, hop],
            pair_recv.at[which, step, hop],
            tp=partner,
        )

    started = []

    def begin(copy):
        copy.start()
        started.append(copy)

    order = [(which, step) for which in range(2) for step in range(1, sp_count)]
    own = [
        pltpu.make_async_copy(sources[which].at[me], place(which, me, lane), own_sem.at[which])
        for which in range(2)
    ]
    for which in range(2):
        own[which].start()
        for step in range(1, sp_count):
            begin(far(which, step))
    arrivals = []
    for which in range(2):
        arrivals += [(which, step) for step in range(sp_count)]
    lag = 2
    for at in range(len(arrivals) + lag):
        if at < len(arrivals):
            which, step = arrivals[at]
            if step:
                far(which, step).wait_recv()
            for hop in range(1, chips):
                begin(beside(which, step, hop))
            begin(paired(which, step, 0))
        if at >= lag:
            which, step = arrivals[at - lag]
            for hop in range(1, chips):
                beside(which, step, hop).wait_recv()
                begin(paired(which, step, hop))
    for which, step in arrivals:
        for hop in range(chips):
            paired(which, step, hop).wait_recv()
    for copy in started:
        copy.wait_send()
    for copy in own:
        copy.wait()


def dispatch(send_rows, send_cot, sp_count, tp_count):
    blocks, capacity, width = send_rows.shape
    full = jax.ShapeDtypeStruct((blocks, capacity, width * tp_count), send_rows.dtype)
    dma = pltpu.SemaphoreType.DMA
    chips = tp_count // 2
    return pl.pallas_call(
        functools.partial(dispatch_kernel, sp_count, tp_count),
        out_shape=(full, full),
        in_specs=[pl.BlockSpec(memory_space=pltpu.VMEM)] * 2,
        out_specs=[pl.BlockSpec(memory_space=pl.ANY)] * 2,
        scratch_shapes=[dma((2, sp_count))] * 2
        + [dma((2, sp_count, chips))] * 4
        + [dma((2,))],
        compiler_params=pltpu.CompilerParams(collective_id=0, has_side_effects=True),
        name="dispatch",
    )(send_rows, send_cot)


def tail_kernel(
    sp_count,
    tp_count,
    partial_ref,
    picks_ref,
    upstream_ref,
    saved_ref,
    proj_ref,
    taps_ref,
    value_ref,
    gate_ref,
    grad_stream_ref,
    grad_value_ref,
    grad_gate_ref,
    grad_proj_ref,
    pair_in,
    side_out,
    side_in,
    total,
    returned,
    full,
    stat_out,
    stat_in,
    parts_out,
    parts_in,
    rim_in,
    padded,
    pair_send,
    pair_recv,
    side_send,
    side_recv,
    far_send,
    far_recv,
    full_send,
    full_recv,
    stat_send,
    stat_recv,
    parts_send,
    parts_recv,
    rim_send,
    rim_recv,
):
    me, lane = lax.axis_index("sp"), lax.axis_index("tp")
    width = returned.shape[2]
    chips = tp_count // 2
    core = lax.rem(lane, 2)
    partner = lane + 1 - 2 * core
    tok_count, channels = saved_ref.shape
    conv_width = channels * tp_count
    groups = tok_count // 128
    f32, bf16 = jnp.float32, jnp.bfloat16

    greet(sp_count, tp_count)
    started = []

    def begin(copy):
        copy.start()
        started.append(copy)

    def columns(column):
        return pl.ds(pl.multiple_of(column * width, width), width)

    def swapped(step, hop):
        block = lax.rem(me + step, sp_count)
        other = lax.rem(lane + 2 * hop, tp_count) + 1 - 2 * core
        return remote(
            partial_ref.at[block, :, columns(other)],
            pair_in.at[step, hop],
            pair_send.at[step, hop],
            pair_recv.at[step, hop],
            tp=partner,
        )

    def beside(step, hop):
        return remote(
            side_out.at[step, hop - 1],
            side_in.at[step, hop - 1],
            side_send.at[step, hop - 1],
            side_recv.at[step, hop - 1],
            tp=lax.rem(lane + 2 * hop, tp_count),
        )

    def far(step):
        return remote(
            total.at[step],
            returned.at[me],
            far_send.at[step],
            far_recv.at[step],
            sp=lax.rem(me + step, sp_count),
        )

    order = list(range(1, sp_count)) + [0]
    for step in order:
        for hop in list(range(1, chips)) + [0]:
            begin(swapped(step, hop))

    eye = (
        lax.broadcasted_iota(jnp.int32, (128, 128), 0)
        == lax.broadcasted_iota(jnp.int32, (128, 128), 1)
    )

    def stat(phase, hop):
        return remote(
            stat_out.at[phase],
            stat_in.at[phase, hop],
            stat_send.at[phase, hop],
            stat_recv.at[phase, hop],
            tp=lax.rem(lane + hop, tp_count),
        )

    def share(phase, sums):
        stat_out[phase] = jnp.zeros(stat_out.shape[1:], f32)
        row = 0
        for item in sums:
            for group in range(groups):
                part = item[group * 128 : (group + 1) * 128]
                spread = jnp.where(eye, jnp.broadcast_to(part, (128, 128)), 0.0)
                stat_out[phase, row : row + 1] = jnp.sum(spread, axis=0, keepdims=True)
                row += 1
        for hop in range(1, tp_count):
            begin(stat(phase, hop))

    def shared(phase):
        value = stat_out[phase]
        for hop in range(1, tp_count):
            stat(phase, hop).wait_recv()
            value += stat_in[phase, hop]
        columns_of = []
        for item in range(2):
            parts = []
            for group in range(groups):
                row = item * groups + group
                spread = jnp.broadcast_to(value[row : row + 1], (128, 128))
                parts.append(jnp.sum(jnp.where(eye, spread, 0.0), axis=1, keepdims=True))
            columns_of.append(jnp.concatenate(parts, axis=0))
        return columns_of

    saved_conv = saved_ref[...].astype(f32)
    share(
        0,
        (
            jnp.sum(saved_conv, axis=1, keepdims=True),
            jnp.sum(saved_conv * saved_conv, axis=1, keepdims=True),
        ),
    )

    def pair_sum(step, hop):
        block = lax.rem(me + step, sp_count)
        column = lax.rem(lane + 2 * hop, tp_count)
        return partial_ref[block, :, columns(column)].astype(f32) + pair_in[step, hop].astype(f32)

    lag = 2
    for at in range(sp_count + lag):
        if at < sp_count:
            step = order[at]
            for hop in range(1, chips):
                swapped(step, hop).wait_recv()
                side_out[step, hop - 1] = pair_sum(step, hop).astype(bf16)
                begin(beside(step, hop))
        if at >= lag:
            step = order[at - lag]
            swapped(step, 0).wait_recv()
            value = pair_sum(step, 0)
            for hop in range(1, chips):
                beside(step, hop).wait_recv()
                value += side_in[step, hop - 1].astype(f32)
            if step:
                total[step] = value.astype(bf16)
                begin(far(step))
            else:
                returned[me] = value.astype(bf16)

    total_sum, square_sum = shared(0)
    mean_c = total_sum / conv_width
    var_c = square_sum / conv_width - mean_c * mean_c
    inv_std = lax.rsqrt(var_c + norm_eps)
    normed = (saved_conv - mean_c) * inv_std
    norm_sigmoid = jax.nn.sigmoid(normed)
    mixed = (normed * norm_sigmoid).astype(bf16)

    for step in range(1, sp_count):
        far(step).wait_recv()
    routed_sum = jnp.dot(
        picks_ref[...],
        returned[...].reshape(-1, width),
        preferred_element_type=f32,
    )
    own_grad = (upstream_ref[...].astype(f32) + routed_sum).astype(bf16)
    grad_stream_ref[...] = own_grad
    full[:, columns(lane)] = own_grad

    def spread_full(hop):
        return remote(
            full.at[:, columns(lane)],
            full.at[:, columns(lane)],
            full_send.at[0, hop],
            full_recv.at[0, hop],
            tp=lax.rem(lane + 2 * hop, tp_count),
        )

    def hand_over(hop):
        column = lax.rem(lane + tp_count - 2 * hop, tp_count)
        return remote(
            full.at[:, columns(column)],
            full.at[:, columns(column)],
            full_send.at[1, hop],
            full_recv.at[1, hop],
            tp=partner,
        )

    for hop in range(1, chips):
        begin(spread_full(hop))
    begin(hand_over(0))
    for hop in range(1, chips):
        spread_full(hop).wait_recv()
        begin(hand_over(hop))
    for hop in range(chips):
        hand_over(hop).wait_recv()

    for column in range(tp_count):
        block = contract_rows(full[:, column * width : (column + 1) * width], mixed)
        per = sp_count // tp_count
        parts_out[column * per : (column + 1) * per] = block.reshape(
            per, width // per, channels
        ).astype(bf16)

    def give_parts(step):
        to = lax.rem(me + step, sp_count)
        return remote(
            parts_out.at[to],
            parts_in.at[step],
            parts_send.at[step],
            parts_recv.at[step],
            sp=to,
        )

    for step in range(1, sp_count):
        begin(give_parts(step))

    grad_mixed = jnp.dot(full[...], proj_ref[...], preferred_element_type=f32)
    grad_normed = grad_mixed * norm_sigmoid * (1.0 + normed * (1.0 - norm_sigmoid))
    share(
        1,
        (
            jnp.sum(grad_normed, axis=1, keepdims=True),
            jnp.sum(grad_normed * normed, axis=1, keepdims=True),
        ),
    )
    first_sum, second_sum = shared(1)
    grad_conv = inv_std * (
        grad_normed - first_sum / conv_width - normed * (second_sum / conv_width)
    )
    padded[:tok_count] = grad_conv
    rim = rim_in.shape[0]
    rim_copy = remote(
        padded.at[pl.ds(0, rim)],
        rim_in,
        rim_send.at[0],
        rim_recv.at[0],
        sp=lax.rem(me + sp_count - 1, sp_count),
    )
    begin(rim_copy)
    gate_sig = jax.nn.sigmoid(gate_ref[...].astype(f32))
    rim_copy.wait_recv()
    padded[tok_count:] = jnp.where(me == sp_count - 1, 0.0, rim_in[...])
    grad_glu = jnp.zeros((tok_count, channels), f32)
    for offset in range(taps_ref.shape[0]):
        grad_glu += taps_ref[offset : offset + 1] * padded[offset : offset + tok_count]
    grad_value_ref[...] = (grad_glu * gate_sig).astype(bf16)
    grad_gate_ref[...] = (
        grad_glu * value_ref[...].astype(f32) * gate_sig * (1.0 - gate_sig)
    ).astype(bf16)

    summed = parts_out[me].astype(f32)
    for step in range(1, sp_count):
        give_parts(step).wait_recv()
        summed += parts_in[step].astype(f32)
    grad_proj_ref[...] = summed
    for copy in started:
        copy.wait_send()


def finish(sp_count, tp_count, partial_rows, picks, upstream_own, *conv_args):
    conv_saved, out_proj, conv_taps = conv_args[:3]
    blocks, capacity, model_width = partial_rows.shape
    tok_count, channels = conv_saved.shape
    width = model_width // tp_count
    chips = tp_count // 2
    rim = -(-(conv_taps.shape[0] - 1) // 8) * 8
    dma, vmem = pltpu.SemaphoreType.DMA, pltpu.VMEM
    f32, bf16 = jnp.float32, jnp.bfloat16
    proj_rows = model_width // sp_count
    shape = jax.ShapeDtypeStruct
    return pl.pallas_call(
        functools.partial(tail_kernel, sp_count, tp_count),
        out_shape=(
            shape((tok_count, width), bf16),
            shape((tok_count, channels), bf16),
            shape((tok_count, channels), bf16),
            shape((proj_rows, channels), f32),
        ),
        in_specs=[pl.BlockSpec(memory_space=vmem)] * 8,
        out_specs=[pl.BlockSpec(memory_space=vmem)] * 4,
        scratch_shapes=[
            vmem((sp_count, chips, capacity, width), bf16),
            vmem((sp_count, chips - 1, capacity, width), bf16),
            vmem((sp_count, chips - 1, capacity, width), bf16),
            vmem((sp_count, capacity, width), bf16),
            vmem((sp_count, capacity, width), bf16),
            vmem((tok_count, model_width), bf16),
            vmem((2, 8, 128), f32),
            vmem((2, tp_count, 8, 128), f32),
            vmem((sp_count, proj_rows, channels), bf16),
            vmem((sp_count, proj_rows, channels), bf16),
            vmem((rim, channels), f32),
            vmem((tok_count + rim, channels), f32),
            dma((sp_count, chips)),
            dma((sp_count, chips)),
            dma((sp_count, chips - 1)),
            dma((sp_count, chips - 1)),
            dma((sp_count,)),
            dma((sp_count,)),
            dma((2, chips)),
            dma((2, chips)),
            dma((2, tp_count)),
            dma((2, tp_count)),
            dma((sp_count,)),
            dma((sp_count,)),
            dma((1,)),
            dma((1,)),
        ],
        compiler_params=pltpu.CompilerParams(collective_id=1, has_side_effects=True),
        name="finish",
    )(partial_rows, picks, upstream_own, *conv_args)


def expert_backward(expert_rows, expert_cot, gate_weight, up_weight, down_weight):
    gate_pre = jnp.dot(expert_rows, gate_weight, preferred_element_type=jnp.float32)
    up_pre = jnp.dot(expert_rows, up_weight, preferred_element_type=jnp.float32)
    capped = jnp.minimum(gate_pre, clamp_limit)
    clipped = jnp.clip(up_pre, -clamp_limit, clamp_limit)
    gate_sigmoid = jax.nn.sigmoid(glu_alpha * capped)
    act = (capped * gate_sigmoid * (clipped + 1.0)).astype(jnp.bfloat16)
    grad_down = contract_rows(act, expert_cot)
    grad_act = times_transposed(expert_cot, down_weight)
    slope = gate_sigmoid + glu_alpha * capped * gate_sigmoid * (1.0 - gate_sigmoid)
    grad_gate_pre = jnp.where(
        gate_pre < clamp_limit, grad_act * (clipped + 1.0) * slope, 0.0
    ).astype(jnp.bfloat16)
    grad_up_pre = jnp.where(
        jnp.abs(up_pre) < clamp_limit, grad_act * capped * gate_sigmoid, 0.0
    ).astype(jnp.bfloat16)
    grad_gate = contract_rows(expert_rows, grad_gate_pre)
    grad_up = contract_rows(expert_rows, grad_up_pre)
    return (grad_gate, grad_up, grad_down, grad_gate_pre, grad_up_pre)


def on_device(
    upstream,
    stream,
    routes,
    route_weights,
    glu_value,
    glu_gate,
    conv_taps,
    conv_saved,
    out_proj,
    expert_gate,
    expert_up,
    expert_down,
):
    tok_count = upstream.shape[0]
    model_width = upstream.shape[1]
    expert_count = lax.axis_size("sp")
    capacity = 4 * tok_count // expert_count
    slice_width = model_width // lax.axis_size("tp")
    column_start = lax.axis_index("tp") * slice_width
    targets = pair_rows(routes, expert_count, capacity)
    picks, row_weights = select_pairs(targets, route_weights, expert_count * capacity)
    stream_part = lax.dynamic_slice_in_dim(stream, column_start, slice_width, 1)
    upstream_part = lax.dynamic_slice_in_dim(upstream, column_start, slice_width, 1)
    send_rows = jnp.dot(picks, stream_part, preferred_element_type=jnp.float32).astype(jnp.bfloat16)
    send_cot = (
        row_weights[:, None] * jnp.dot(picks, upstream_part, preferred_element_type=jnp.float32)
    ).astype(jnp.bfloat16)
    part_shape = (expert_count, capacity, slice_width)
    got_rows, got_cot = dispatch(
        send_rows.reshape(part_shape),
        send_cot.reshape(part_shape),
        expert_count,
        lax.axis_size("tp"),
    )
    expert_rows = got_rows.reshape(-1, model_width)
    expert_cot = got_cot.reshape(-1, model_width)
    gate_weight = expert_gate[0]
    up_weight = expert_up[0]
    down_weight = expert_down[0]
    grad_gate_w, grad_up_w, grad_down_w, grad_gate_pre, grad_up_pre = expert_backward(
        expert_rows, expert_cot, gate_weight, up_weight, down_weight
    )
    partial_rows = times_transposed(grad_gate_pre, gate_weight) + times_transposed(
        grad_up_pre, up_weight
    )
    grad_stream, grad_value, grad_gate, grad_out_proj = finish(
        expert_count,
        lax.axis_size("tp"),
        partial_rows.astype(jnp.bfloat16).reshape(expert_count, capacity, model_width),
        picks.T,
        upstream_part,
        conv_saved,
        out_proj,
        conv_taps,
        glu_value,
        glu_gate,
    )
    return (
        grad_stream,
        grad_value,
        grad_gate,
        grad_out_proj,
        grad_gate_w[None],
        grad_up_w[None],
        grad_down_w[None],
    )


def solution(mesh):
    in_specs = (
        P("sp", None),
        P("sp", None),
        P("sp", None),
        P("sp", None),
        P("sp", "tp"),
        P("sp", "tp"),
        P(None, "tp"),
        P("sp", "tp"),
        P(None, "tp"),
        P("sp", None, "tp"),
        P("sp", None, "tp"),
        P("sp", "tp", None),
    )
    out_specs = (
        P("sp", "tp"),
        P("sp", "tp"),
        P("sp", "tp"),
        P("sp", "tp"),
        P("sp", None, "tp"),
        P("sp", None, "tp"),
        P("sp", "tp", None),
    )
    return jax.shard_map(
        on_device, mesh=mesh, in_specs=in_specs, out_specs=out_specs, check_vma=False
    )
```

profile of v0, /device:TPU:23, one launch (start us, length us, event | category | flops | bytes accessed | tf_op | source)
XLA Modules:
  0.0 178.2 jit_solution(12313620134751769936)
XLA Ops:
  0.6 0.0 copy-start
  0.6 0.9 fusion.27
  1.5 0.2 select_reduce_fusion.1
  1.7 0.8 fusion.26
  2.5 0.3 add_reduce_fusion
  2.8 1.0 constant_dynamic-slice_fusion.upstream_ref
  3.8 0.0 copy-start.1
  3.8 1.4 multiply_convert_fusion.1
  5.2 2.4 %convolution_convert_fusion = bf16[1024,512]{1,0:T(8,128)(2,1)} fusion(s32[256]{0:T(256)S(1)} %get-tuple-element.27, s32[256]{0:T(256)S(1)} %get-tuple-element.28, bf16[256,2048]{1,0:T(8,128)(2,1)} %param.13, s32[]{:T(128)S(6)} %select_n.18), kind=kOutput, calls=%fused_computation.20 | convolution fusion | flops 270532608 | bytes 1312772 | tf_op jit(solution)/shard_map/dot_general | solution.py:582
  7.6 65.4 %dispatch.1 = (bf16[8,128,2048]{2,1,0:T(8,128)(2,1)}, bf16[8,128,2048]{2,1,0:T(8,128)(2,1)}) custom-call(bf16[8,128,512]{2,1,0:T(8,128)(2,1)} %bitcast.43, bf16[8,128,512]{2,1,0:T(8,128)(2,1)} %bitcast.42), custom_call_target="tpu_custom_call" | custom-call | tf_op jit(solution)/shard_map/dispatch/pallas_call | solution.py:188
  73.0 0.0 copy-done.1
  73.0 0.0 copy-start.2
  73.0 5.3 %fusion.1 = f32[1024,512]{1,0:T(8,128)S(1)} fusion(bf16[1024,2048]{1,0:T(8,128)(2,1)} %bitcast.50, bf16[1,2048,512]{2,1,0:T(8,128)(2,1)} %param.22), kind=kOutput, calls=%fused_computation.5 | convolution fusion | flops 2147483648 | bytes 8388608 | tf_op jit(solution)/shard_map/dot_general | solution.py:539
  78.3 0.0 copy-done
  78.3 0.0 copy-done.2
  78.4 0.0 copy-start.3
  78.4 2.3 %fusion.7 = f32[1024,512]{1,0:T(8,128)S(1)} fusion(bf16[1024,2048]{1,0:T(8,128)(2,1)S(1)} %bitcast.51, bf16[1,2048,512]{2,1,0:T(8,128)(2,1)S(1)} %copy-done), kind=kOutput, calls=%fused_computation.11 | convolution fusion | flops 2147483648 | bytes 8388608 | tf_op jit(solution)/shard_map/dot_general | solution.py:538
  80.7 0.0 copy-done.3
  80.7 0.0 copy-start.4
  80.7 4.8 %convolution_bitcast_fusion = f32[1,512,2048]{2,1,0:T(8,128)} fusion(bf16[1024,2048]{1,0:T(8,128)(2,1)S(1)} %bitcast.54, f32[1024,512]{1,0:T(8,128)S(1)} %fusion.7, f32[1024,512]{1,0:T(8,128)S(1)} %fusion.1), kind=kOutput, calls=%fused_computation.1 | convolution fusion | flops 2152726528 | bytes 12582912 | tf_op jit(solution)/shard_map/dot_general | solution.py:17
  85.5 0.0 copy-done.4
  85.5 3.6 %select_convert_fusion = (bf16[1024,512]{1,0:T(8,128)(2,1)S(1)}, bf16[1024,512]{1,0:T(8,128)(2,1)S(1)}) fusion(f32[1024,512]{1,0:T(8,128)S(1)} %fusion.1, f32[1024,512]{1,0:T(8,128)S(1)} %fusion.7, bf16[1024,2048]{1,0:T(8,128)(2,1)S(1)} %bitcast.55, bf16[1,512,2048]{2,1,0:T(8,128)(2,1)S(1)} %copy-done.4), kind=kOutput, calls=%fused_computation.14 | convolution fusion | flops 2159017984 | bytes 12582912 | tf_op jit(solution)/shard_map/dot_general | solution.py:23
  89.1 4.7 %convolution_bitcast_fusion.1 = f32[1,2048,512]{2,1,0:T(8,128)} fusion(bf16[1024,2048]{1,0:T(8,128)(2,1)S(1)} %bitcast.52, bf16[1024,512]{1,0:T(8,128)(2,1)S(1)} %get-tuple-element.21), kind=kOutput, calls=%fused_computation.2 | convolution fusion | flops 2147483648 | bytes 9437184 | tf_op jit(solution)/shard_map/dot_general | solution.py:17
  93.8 4.5 %convolution_bitcast_fusion.2 = f32[1,2048,512]{2,1,0:T(8,128)} fusion(bf16[1024,2048]{1,0:T(8,128)(2,1)S(1)} %bitcast.53, bf16[1024,512]{1,0:T(8,128)(2,1)S(1)} %get-tuple-element.22), kind=kOutput, calls=%fused_computation.3 | convolution fusion | flops 2147483648 | bytes 9437184 | tf_op jit(solution)/shard_map/dot_general | solution.py:17
  98.3 2.4 %fusion.5 = f32[1024,2048]{1,0:T(8,128)S(1)} fusion(bf16[1024,512]{1,0:T(8,128)(2,1)S(1)} %get-tuple-element.22, bf16[1,2048,512]{2,1,0:T(8,128)(2,1)S(1)} %copy-done), kind=kOutput, calls=%fused_computation.9 | convolution fusion | flops 2147483648 | bytes 11534336 | tf_op jit(solution)/shard_map/dot_general | solution.py:23
  100.6 4.3 %add_convert_fusion = bf16[1024,2048]{1,0:T(8,128)(2,1)} fusion(f32[1024,2048]{1,0:T(8,128)S(1)} %fusion.5, bf16[1024,512]{1,0:T(8,128)(2,1)S(1)} %get-tuple-element.21, bf16[1,2048,512]{2,1,0:T(8,128)(2,1)S(1)} %copy-done.5), kind=kOutput, calls=%fused_computation | convolution fusion | flops 2151677952 | bytes 15728640 | tf_op jit(solution)/shard_map/dot_general | solution.py:23
  105.0 1.1 add_convert_fusion.1.picks_ref
  106.0 65.9 %finish.1 = (bf16[256,512]{1,0:T(8,128)(2,1)}, bf16[256,128]{1,0:T(8,128)(2,1)}, bf16[256,128]{1,0:T(8,128)(2,1)}, f32[256,128]{1,0:T(8,128)}) custom-call(bf16[8,128,2048]{2,1,0:T(8,128)(2,1)} %bitcast.41, bf16[256,1024]{1,0:T(8,128)(2,1)} %add_convert_fusion.1.picks_ref, bf16[256,512]{1,0:T(8,128)(2,1)} %copy-done.1, bf16[256,128]{1,0:T(8,128)(2,1)} %saved_ref.1, ...), custom_call_target="tpu_custom_call" | custom-call | tf_op jit(solution)/shard_map/finish/pallas_call | solution.py:494
  172.0 1.7 copy.23
  173.7 1.5 copy.24
  175.1 1.5 copy.25
  176.6 1.6 copy.26
  (3 shorter events, 0.0 us)
Async XLA Ops:
  0.6 77.7 %copy-start = (bf16[1,2048,512]{2,1,0:T(8,128)(2,1)S(1)}, bf16[1,2048,512]{2,1,0:T(8,128)(2,1)}, u32[]{:S(2)}) copy-start(bf16[1,2048,512]{2,1,0:T(8,128)(2,1)} %param.21) | copy-start | bytes 6291460
  3.8 69.2 %copy-start.1 = (bf16[256,512]{1,0:T(8,128)(2,1)}, bf16[256,512]{1,0:T(8,128)(2,1)S(1)}, u32[]{:S(2)}) copy-start(bf16[256,512]{1,0:T(8,128)(2,1)S(1)} %constant_dynamic-slice_fusion.upstream_ref) | copy-start | bytes 786436
  73.0 5.3 %copy-start.2 = (bf16[8,128,2048]{2,1,0:T(8,128)(2,1)S(1)}, bf16[8,128,2048]{2,1,0:T(8,128)(2,1)}, u32[]{:S(2)}) copy-start(bf16[8,128,2048]{2,1,0:T(8,128)(2,1)} %get-tuple-element.13) | copy-start | bytes 12582916
  78.4 2.3 %copy-start.3 = (bf16[8,128,2048]{2,1,0:T(8,128)(2,1)S(1)}, bf16[8,128,2048]{2,1,0:T(8,128)(2,1)}, u32[]{:S(2)}) copy-start(bf16[8,128,2048]{2,1,0:T(8,128)(2,1)} %get-tuple-element.14) | copy-start | bytes 12582916
  80.7 4.8 %copy-start.4 = (bf16[1,512,2048]{2,1,0:T(8,128)(2,1)S(1)}, bf16[1,512,2048]{2,1,0:T(8,128)(2,1)}, u32[]{:S(2)}) copy-start(bf16[1,512,2048]{2,1,0:T(8,128)(2,1)} %param.23) | copy-start | bytes 6291460
  98.3 2.4 %copy-start.5 = (bf16[1,2048,512]{2,1,0:T(8,128)(2,1)S(1)}, bf16[1,2048,512]{2,1,0:T(8,128)(2,1)}, u32[]{:S(2)}) copy-start(bf16[1,2048,512]{2,1,0:T(8,128)(2,1)} %param.22) | copy-start | bytes 6291460
where the time goes:
time: 182 us; the launch traced here: 178 us
  Pallas kernels  131 us (72%)
  matrix products  35.9 us (20%)
  local copies, waits for them, and re-layouts  8.8 us (5%)
    pallas_call x1, Pallas kernels, finish(): pl.pallas_call(functools.partial(tail_kernel, sp_count, tp_count), out_sh...  65.9 us
    pallas_call x1, Pallas kernels, dispatch(): pl.pallas_call(functools.partial(dispatch_kernel, sp_count, tp_count), ou...  65.4 us
    dot_general x3, matrix products, contract_rows(): lax.dot_general(left, right, (((0,), (0,)), ((), ())), preferred_element_...  13.9 us
    dot_general x3, matrix products, times_transposed(): lax.dot_general(left, right, (((1,), (1,)), ((), ())), preferred_element_...  10.3 us
    unnamed x16, local copies, waits for them, and re-layouts  6.22 us
    dot_general x1, matrix products, expert_backward(): up_pre = jnp.dot(expert_rows, up_weight, preferred_element_type=jnp.float32)  5.32 us

commit v1 on v0

v1 whole, which is shorter than its diff:
```python
import functools

import jax
import jax.numpy as jnp
from jax import lax
from jax.experimental import pallas as pl
from jax.experimental.pallas import tpu as pltpu
from jax.sharding import PartitionSpec as P


clamp_limit = 7.0
glu_alpha = 1.702
norm_eps = 1e-05


def contract_rows(left, right):
    return lax.dot_general(
        left, right, (((0,), (0,)), ((), ())), preferred_element_type=jnp.float32
    )


def times_transposed(left, right):
    return lax.dot_general(
        left, right, (((1,), (1,)), ((), ())), preferred_element_type=jnp.float32
    )


def greet(sp_count, tp_count):
    me, lane = lax.axis_index("sp"), lax.axis_index("tp")
    barrier = pltpu.get_barrier_semaphore()
    for step in range(1, sp_count):
        pl.semaphore_signal(
            barrier,
            inc=1,
            device_id={"sp": lax.rem(me + step, sp_count)},
            device_id_type=pl.DeviceIdType.MESH,
        )
    for step in range(1, tp_count):
        pl.semaphore_signal(
            barrier,
            inc=1,
            device_id={"tp": lax.rem(lane + step, tp_count)},
            device_id_type=pl.DeviceIdType.MESH,
        )
    pl.semaphore_wait(barrier, sp_count + tp_count - 2)


def remote(src, dst, send_sem, recv_sem, **target):
    return pltpu.make_async_remote_copy(
        src_ref=src,
        dst_ref=dst,
        send_sem=send_sem,
        recv_sem=recv_sem,
        device_id=target,
        device_id_type=pl.DeviceIdType.MESH,
    )


def load_in(src, dst, sem):
    return pltpu.make_async_copy(src, dst, sem)


def fused_kernel(
    sp_count,
    tp_count,
    meta_ref,
    stream_hbm,
    upstream_hbm,
    gate_hbm,
    up_hbm,
    down_hbm,
    saved_hbm,
    proj_hbm,
    taps_hbm,
    value_hbm,
    conv_gate_hbm,
    grad_stream_ref,
    grad_value_ref,
    grad_gate_ref,
    grad_proj_ref,
    gate_out,
    up_out,
    down_out,
    tokens,
    weights,
    down_ref,
    saved_ref,
    proj_ref,
    taps_ref,
    value_ref,
    gate_ref,
    metas,
    chained,
    both,
    chosen,
    gains,
    near_out,
    cross_out,
    before,
    picks_all,
    picks_t,
    act_t,
    slopes,
    partial,
    pair_in,
    side_out,
    side_in,
    total,
    returned,
    full,
    stat_out,
    stat_in,
    parts_out,
    parts_in,
    rim_in,
    padded,
    gate_acc,
    up_acc,
    down_acc,
    load_sem,
    store_sem,
    meta_send,
    meta_recv,
    chain_send,
    chain_recv,
    cross_send,
    cross_recv,
    along_send,
    along_recv,
    twin_send,
    twin_recv,
    pair_send,
    pair_recv,
    side_send,
    side_recv,
    far_send,
    far_recv,
    full_send,
    full_recv,
    stat_send,
    stat_recv,
    parts_send,
    parts_recv,
    rim_send,
    rim_recv,
):
    me, lane = lax.axis_index("sp"), lax.axis_index("tp")
    chips = tp_count // 2
    across = chips
    layers = sp_count // across
    layer, place = lax.div(me, across), lax.rem(me, across)
    core = lax.rem(lane, 2)
    partner = lane + 1 - 2 * core
    tok_count, model_width = tokens.shape[1:]
    capacity = both.shape[2]
    width = model_width // tp_count
    hidden = down_ref.shape[0]
    group_rows = across * capacity
    channels = saved_ref.shape[1]
    conv_width = channels * tp_count
    groups = tok_count // 128
    f32, bf16 = jnp.float32, jnp.bfloat16

    loads = [
        load_in(stream_hbm, tokens.at[0], load_sem.at[0]),
        load_in(upstream_hbm, tokens.at[1], load_sem.at[1]),
        load_in(saved_hbm, saved_ref, load_sem.at[2]),
        load_in(gate_hbm.at[0], weights.at[:, pl.ds(0, hidden)], load_sem.at[3]),
        load_in(up_hbm.at[0], weights.at[:, pl.ds(hidden, hidden)], load_sem.at[4]),
        load_in(down_hbm.at[0], down_ref, load_sem.at[5]),
        load_in(proj_hbm, proj_ref, load_sem.at[6]),
        load_in(taps_hbm, taps_ref, load_sem.at[7]),
        load_in(value_hbm, value_ref, load_sem.at[8]),
        load_in(conv_gate_hbm, gate_ref, load_sem.at[9]),
    ]
    for load in loads:
        load.start()

    before[...] = jnp.where(
        lax.broadcasted_iota(jnp.int32, before.shape, 0)
        < lax.broadcasted_iota(jnp.int32, before.shape, 1),
        1.0,
        0.0,
    ).astype(bf16)

    greet(sp_count, tp_count)
    started = []

    def begin(copy):
        copy.start()
        started.append(copy)

    def columns(column):
        return pl.ds(pl.multiple_of(column * width, width), width)

    def layer_at(step):
        if step == 0:
            return layer
        inner = jnp.minimum(layer, layers - 1 - layer)
        paired = step <= 2 * inner
        reach = jnp.where(paired, (step + 1) // 2, step - inner)
        below = jnp.where(paired, step % 2 == 1, layer > layers - 1 - layer)
        return jnp.where(below, layer - reach, layer + reach)

    at_layer = [layer_at(step) for step in range(layers)]

    def block_at(step, index):
        return at_layer[step] * across + lax.rem(place + across - index, across)

    def give_meta(step):
        return remote(
            meta_ref,
            metas.at[layer],
            meta_send.at[step],
            meta_recv.at[layer],
            sp=lax.rem(me + step * across, sp_count),
        )

    for step in range(1, layers):
        begin(give_meta(step))

    def own_chain(which, up):
        to = me + across if up else me + sp_count - across
        return remote(
            tokens.at[which, :, columns(lane)],
            chained.at[which, layer],
            chain_send.at[which, 0, int(up)],
            chain_recv.at[which, layer],
            sp=lax.rem(to, sp_count),
        )

    def chain_on(which, step):
        source = at_layer[step]
        to = jnp.where(source < layer, me + across, me + sp_count - across)
        return remote(
            chained.at[which, source],
            chained.at[which, source],
            chain_send.at[which, step, 0],
            chain_recv.at[which, source],
            sp=lax.rem(to, sp_count),
        )

    def goes_on(step):
        source = at_layer[step]
        return jnp.where(source < layer, layer < layers - 1, layer > 0)

    for which in range(2):
        loads[which].wait()

        @pl.when(layer < layers - 1)
        def _():
            own_chain(which, True).start()

        @pl.when(layer > 0)
        def _():
            own_chain(which, False).start()

    def piece(which, block, column):
        return both.at[which, block, :, columns(column)]

    def column_at(hop):
        return lax.rem(lane + tp_count - 2 * hop, tp_count)

    def cross(which, step, index, hop):
        column = column_at(hop)
        source = near_out.at[which, index - 1, hop] if step == 0 else cross_out.at[which, step - 1, index - 1]
        return remote(
            source,
            piece(which, block_at(step, 0), column),
            cross_send.at[which, step, index - 1, hop],
            cross_recv.at[which, step, index - 1, hop],
            sp=layer * across + lax.rem(place + index, across),
        )

    def along(which, step, index, hop):
        here = piece(which, block_at(step, index), lane)
        return remote(
            here,
            here,
            along_send.at[which, step, index, hop - 1],
            along_recv.at[which, step, index, hop - 1],
            tp=lax.rem(lane + 2 * hop, tp_count),
        )

    def twin(which, step, index, hop):
        here = piece(which, block_at(step, index), column_at(hop))
        return remote(
            here,
            here,
            twin_send.at[which, step, index, hop],
            twin_recv.at[which, step, index, hop],
            tp=partner,
        )

    def choose(meta):
        rows = lax.broadcasted_iota(jnp.int32, (8, tok_count), 0) + place
        rows = jnp.where(rows >= across, rows - across, rows) + layer * across
        names = rows.astype(f32)
        hit = jnp.where((meta[0:1] == names) | (meta[1:2] == names), 1.0, 0.0)
        slots = jnp.dot(hit.astype(bf16), before[...], preferred_element_type=f32)
        slot_rows = lax.broadcasted_iota(jnp.int32, (capacity, tok_count), 0).astype(f32)
        for index in range(across):
            pick = jnp.where(
                (slots[index : index + 1] == slot_rows) & (hit[index : index + 1] > 0.0), 1.0, 0.0
            )
            chosen[index] = pick.astype(bf16)
            gain = jnp.where(meta[0:1] == names[index : index + 1], meta[2:3], meta[3:4])
            row_gain = jnp.sum(pick * gain, axis=1, keepdims=True)
            gains[index] = jnp.broadcast_to(row_gain, (capacity, 128))

    def picked(which, index, source):
        rows = jnp.dot(chosen[index], source, preferred_element_type=f32)
        if which == 1:
            rows = rows * gains[index][:, :1]
        return rows.astype(bf16)

    def stage_forward(step):
        @pl.when(goes_on(step))
        def _():
            for which in range(2):
                chain_on(which, step).wait_recv()
                chain_on(which, step).start()

    def stage_select(step):
        if step == 0:
            choose(meta_ref[...])
            for which in range(2):
                for index in range(1, across):
                    for hop in range(chips):
                        near_out[which, index - 1, hop] = picked(
                            which, index, tokens[which, :, columns(column_at(hop))]
                        )
                        begin(cross(which, 0, index, hop))
            for which in range(2):
                for column in range(tp_count):
                    both[which, me, :, column * width : (column + 1) * width] = picked(
                        which, 0, tokens[which, :, column * width : (column + 1) * width]
                    )
            return
        source = at_layer[step]
        remote(
            meta_ref, metas.at[source], meta_send.at[0], meta_recv.at[source], sp=lax.rem(me + across, sp_count)
        ).wait_recv()
        choose(metas[source])
        for which in range(2):

            @pl.when(jnp.logical_not(goes_on(step)))
            def _():
                chain_on(which, step).wait_recv()

            for index in range(1, across):
                cross_out[which, step - 1, index - 1] = picked(which, index, chained[which, source])
                begin(cross(which, step, index, 0))
            both[which, block_at(step, 0), :, columns(lane)] = picked(which, 0, chained[which, source])
            for hop in range(1, chips):
                begin(along(which, step, 0, hop))
            begin(twin(which, step, 0, 0))

    def stage_cross(step):
        for which in range(2):
            for index in range(1, across):
                for hop in range(chips if step == 0 else 1):
                    cross(which, step, index, hop).wait_recv()
                    if step:
                        for side in range(1, chips):
                            begin(along(which, step, index, side))
                    begin(twin(which, step, index, hop))

    def stage_along(step):
        if step == 0:
            return
        for which in range(2):
            for index in range(across):
                for hop in range(1, chips):
                    along(which, step, index, hop).wait_recv()
                    begin(twin(which, step, index, hop))

    def group_at(step):
        return pl.ds(at_layer[step] * across, across)

    hidden_tile = min(hidden, 256)

    def stage_expert(step):
        for which in range(2):
            for index in range(across):
                if step or index:
                    for hop in range(chips):
                        twin(which, step, index, hop).wait_recv()
        if step == 0:
            for load in loads[3:6]:
                load.wait()
        first = pl.multiple_of(at_layer[step] * group_rows, group_rows)
        rows_at = pl.ds(first, group_rows)

        @pl.loop(0, hidden // hidden_tile)
        def _(tile):
            units = pl.ds(pl.multiple_of(tile * hidden_tile, hidden_tile), hidden_tile)
            up_units = pl.ds(pl.multiple_of(hidden + tile * hidden_tile, hidden_tile), hidden_tile)
            rows = both[0, group_at(step)].reshape(group_rows, model_width)
            cot = both[1, group_at(step)].reshape(group_rows, model_width)
            gate_pre = jnp.dot(rows, weights[:, units], preferred_element_type=f32)
            up_pre = jnp.dot(rows, weights[:, up_units], preferred_element_type=f32)
            grad_act = times_transposed(cot, down_ref[units, :])
            capped = jnp.minimum(gate_pre, clamp_limit)
            clipped = jnp.clip(up_pre, -clamp_limit, clamp_limit)
            sig = jax.nn.sigmoid(glu_alpha * capped)
            gated = capped * sig
            act_t[units, rows_at] = (gated * (clipped + 1.0)).T.astype(bf16)
            slope = sig + glu_alpha * gated * (1.0 - sig)
            slopes[rows_at, units] = jnp.where(
                gate_pre < clamp_limit, grad_act * (clipped + 1.0) * slope, 0.0
            ).astype(bf16)
            slopes[rows_at, up_units] = jnp.where(
                jnp.abs(up_pre) < clamp_limit, grad_act * gated, 0.0
            ).astype(bf16)

        @pl.loop(0, tp_count)
        def _(tile):
            value = times_transposed(slopes[rows_at, :], weights[columns(tile), :])
            partial[group_at(step), :, columns(tile)] = value.astype(bf16).reshape(
                across, capacity, width
            )

        for hop in list(range(1, chips)) + [0]:
            begin(swapped(step, hop))

    def swapped(step, hop):
        other = lax.rem(lane + 2 * hop, tp_count) + 1 - 2 * core
        return remote(
            partial.at[group_at(step), :, columns(other)],
            pair_in.at[step, hop],
            pair_send.at[step, hop],
            pair_recv.at[step, hop],
            tp=partner,
        )

    def beside(step, hop):
        return remote(
            side_out.at[step, hop - 1],
            side_in.at[step, hop - 1],
            side_send.at[step, hop - 1],
            side_recv.at[step, hop - 1],
            tp=lax.rem(lane + 2 * hop, tp_count),
        )

    def pair_sum(step, hop):
        column = lax.rem(lane + 2 * hop, tp_count)
        return partial[group_at(step), :, columns(column)].astype(f32) + pair_in[step, hop].astype(f32)

    def stage_pair(step):
        for hop in range(1, chips):
            swapped(step, hop).wait_recv()
            side_out[step, hop - 1] = pair_sum(step, hop).astype(bf16)
            begin(beside(step, hop))

    def stage_return(step):
        swapped(step, 0).wait_recv()
        value = pair_sum(step, 0)
        for hop in range(1, chips):
            beside(step, hop).wait_recv()
            value += side_in[step, hop - 1].astype(f32)
        total[step] = value.astype(bf16)
        for index in range(across):
            spot = lax.rem(place + index, across)
            if step == 0 and index == 0:
                returned[me] = total[0, spot]
            else:
                begin(
                    remote(
                        total.at[step, spot],
                        returned.at[me],
                        far_send.at[step, index],
                        far_recv.at[me],
                        sp=at_layer[step] * across + spot,
                    )
                )

    stage_select(0)

    eye = (
        lax.broadcasted_iota(jnp.int32, (128, 128), 0)
        == lax.broadcasted_iota(jnp.int32, (128, 128), 1)
    )

    def stat(phase, hop):
        return remote(
            stat_out.at[phase],
            stat_in.at[phase, hop],
            stat_send.at[phase, hop],
            stat_recv.at[phase, hop],
            tp=lax.rem(lane + hop, tp_count),
        )

    def share(phase, sums):
        stat_out[phase] = jnp.zeros(stat_out.shape[1:], f32)
        row = 0
        for item in sums:
            for group in range(groups):
                part = item[group * 128 : (group + 1) * 128]
                spread = jnp.where(eye, jnp.broadcast_to(part, (128, 128)), 0.0)
                stat_out[phase, row : row + 1] = jnp.sum(spread, axis=0, keepdims=True)
                row += 1
        for hop in range(1, tp_count):
            begin(stat(phase, hop))

    def shared(phase):
        value = stat_out[phase]
        for hop in range(1, tp_count):
            stat(phase, hop).wait_recv()
            value += stat_in[phase, hop]
        columns_of = []
        for item in range(2):
            parts = []
            for group in range(groups):
                row = item * groups + group
                spread = jnp.broadcast_to(value[row : row + 1], (128, 128))
                parts.append(jnp.sum(jnp.where(eye, spread, 0.0), axis=1, keepdims=True))
            columns_of.append(jnp.concatenate(parts, axis=0))
        return columns_of

    loads[2].wait()
    first_conv = saved_ref[...].astype(f32)
    share(
        0,
        (
            jnp.sum(first_conv, axis=1, keepdims=True),
            jnp.sum(first_conv * first_conv, axis=1, keepdims=True),
        ),
    )

    own_meta = meta_ref[...]
    names = lax.broadcasted_iota(jnp.int32, (sp_count, tok_count), 0).astype(f32)
    hit = jnp.where((own_meta[0:1] == names) | (own_meta[1:2] == names), 1.0, 0.0)
    slots = jnp.dot(hit.astype(bf16), before[...], preferred_element_type=f32)
    slot_rows = lax.broadcasted_iota(jnp.int32, (capacity, tok_count), 0).astype(f32)
    for expert in range(sp_count):
        pick = jnp.where(
            (slots[expert : expert + 1] == slot_rows) & (hit[expert : expert + 1] > 0.0), 1.0, 0.0
        )
        picks_all[expert * capacity : (expert + 1) * capacity] = pick.astype(bf16)
    picks_t[...] = picks_all[...].astype(f32).T.astype(bf16)

    if layers > 1:
        stage_forward(1)
        stage_select(1)
    if layers > 2:
        stage_forward(2)
    stage_cross(0)
    stage_expert(0)
    stage_pair(0)
    for step in range(2, layers + 1):
        stage_cross(step - 1)
        if step < layers:
            stage_select(step)
        if step + 1 < layers:
            stage_forward(step + 1)
        stage_along(step - 1)
        stage_expert(step - 1)
        stage_return(step - 2)
        stage_pair(step - 1)

    tile_width = 256
    tiles = model_width // tile_width
    rows_total = sp_count * capacity

    def down_store(tile):
        at = pl.ds(pl.multiple_of(tile * tile_width, tile_width), tile_width)
        return pltpu.make_async_copy(down_acc.at[:, at], down_out.at[0, :, at], store_sem.at[0, tile])

    def gate_store(tile):
        at = pl.ds(pl.multiple_of(tile * tile_width, tile_width), tile_width)
        return pltpu.make_async_copy(gate_acc.at[at], gate_out.at[0, at], store_sem.at[1, tile])

    def up_store(tile):
        at = pl.ds(pl.multiple_of(tile * tile_width, tile_width), tile_width)
        return pltpu.make_async_copy(up_acc.at[at], up_out.at[0, at], store_sem.at[2, tile])

    @pl.loop(0, tiles)
    def _(tile):
        at = pl.ds(pl.multiple_of(tile * tile_width, tile_width), tile_width)
        down_acc[:, at] = jnp.dot(
            act_t[...], both[1, :, :, at].reshape(rows_total, tile_width), preferred_element_type=f32
        )
        down_store(tile).start()

    stage_return(layers - 1)

    @pl.loop(0, tiles)
    def _(tile):
        at = pl.ds(pl.multiple_of(tile * tile_width, tile_width), tile_width)
        left = both[0, :, :, at].reshape(rows_total, tile_width)
        gate_acc[at] = contract_rows(left, slopes[:, :hidden])
        up_acc[at] = contract_rows(left, slopes[:, hidden:])
        gate_store(tile).start()
        up_store(tile).start()

    total_sum, square_sum = shared(0)
    mean_c = total_sum / conv_width
    var_c = square_sum / conv_width - mean_c * mean_c
    inv_std = lax.rsqrt(var_c + norm_eps)
    saved_conv = saved_ref[...].astype(f32)
    normed = (saved_conv - mean_c) * inv_std
    norm_sigmoid = jax.nn.sigmoid(normed)
    mixed = (normed * norm_sigmoid).astype(bf16)
    for load in loads[6:]:
        load.wait()

    for step in range(1, sp_count):
        source = lax.rem(me + step, sp_count)
        remote(
            total.at[0, 0], returned.at[source], far_send.at[0, 0], far_recv.at[source], sp=source
        ).wait_recv()
    routed_sum = jnp.dot(
        picks_t[...],
        returned[...].reshape(-1, width),
        preferred_element_type=f32,
    )
    own_grad = (tokens[1, :, columns(lane)].astype(f32) + routed_sum).astype(bf16)
    grad_stream_ref[...] = own_grad
    full[:, columns(lane)] = own_grad

    def spread_full(hop):
        return remote(
            full.at[:, columns(lane)],
            full.at[:, columns(lane)],
            full_send.at[0, hop],
            full_recv.at[0, hop],
            tp=lax.rem(lane + 2 * hop, tp_count),
        )

    def hand_over(hop):
        column = lax.rem(lane + tp_count - 2 * hop, tp_count)
        return remote(
            full.at[:, columns(column)],
            full.at[:, columns(column)],
            full_send.at[1, hop],
            full_recv.at[1, hop],
            tp=partner,
        )

    for hop in range(1, chips):
        begin(spread_full(hop))
    begin(hand_over(0))
    for hop in range(1, chips):
        spread_full(hop).wait_recv()
        begin(hand_over(hop))
    for hop in range(chips):
        hand_over(hop).wait_recv()

    for column in range(tp_count):
        block = contract_rows(full[:, column * width : (column + 1) * width], mixed)
        per = sp_count // tp_count
        parts_out[column * per : (column + 1) * per] = block.reshape(
            per, width // per, channels
        ).astype(bf16)

    def give_parts(step):
        to = lax.rem(me + step, sp_count)
        return remote(
            parts_out.at[to],
            parts_in.at[step],
            parts_send.at[step],
            parts_recv.at[step],
            sp=to,
        )

    for step in range(1, sp_count):
        begin(give_parts(step))

    grad_mixed = jnp.dot(full[...], proj_ref[...], preferred_element_type=f32)
    grad_normed = grad_mixed * norm_sigmoid * (1.0 + normed * (1.0 - norm_sigmoid))
    share(
        1,
        (
            jnp.sum(grad_normed, axis=1, keepdims=True),
            jnp.sum(grad_normed * normed, axis=1, keepdims=True),
        ),
    )
    first_sum, second_sum = shared(1)
    grad_conv = inv_std * (
        grad_normed - first_sum / conv_width - normed * (second_sum / conv_width)
    )
    padded[:tok_count] = grad_conv
    rim = rim_in.shape[0]
    rim_copy = remote(
        padded.at[pl.ds(0, rim)],
        rim_in,
        rim_send.at[0],
        rim_recv.at[0],
        sp=lax.rem(me + sp_count - 1, sp_count),
    )
    begin(rim_copy)
    gate_sig = jax.nn.sigmoid(gate_ref[...].astype(f32))
    rim_copy.wait_recv()
    padded[tok_count:] = jnp.where(me == sp_count - 1, 0.0, rim_in[...])
    grad_glu = jnp.zeros((tok_count, channels), f32)
    for offset in range(taps_ref.shape[0]):
        grad_glu += taps_ref[offset : offset + 1] * padded[offset : offset + tok_count]
    grad_value_ref[...] = (grad_glu * gate_sig).astype(bf16)
    grad_gate_ref[...] = (
        grad_glu * value_ref[...].astype(f32) * gate_sig * (1.0 - gate_sig)
    ).astype(bf16)

    summed = parts_out[me].astype(f32)
    for step in range(1, sp_count):
        give_parts(step).wait_recv()
        summed += parts_in[step].astype(f32)
    grad_proj_ref[...] = summed

    @pl.loop(0, tiles)
    def _(tile):
        down_store(tile).wait()
        gate_store(tile).wait()
        up_store(tile).wait()

    for copy in started:
        copy.wait_send()
    for which in range(2):

        @pl.when(layer < layers - 1)
        def _():
            own_chain(which, True).wait_send()

        @pl.when(layer > 0)
        def _():
            own_chain(which, False).wait_send()

        for step in range(1, layers):

            @pl.when(goes_on(step))
            def _():
                chain_on(which, step).wait_send()


def fused(sp_count, tp_count, capacity, meta, stream, upstream, gate_w, up_w, down_w, *conv_args):
    conv_saved, out_proj, conv_taps = conv_args[:3]
    tok_count, model_width = stream.shape
    channels = conv_saved.shape[1]
    hidden = down_w.shape[1]
    width = model_width // tp_count
    chips = tp_count // 2
    across = chips
    layers = sp_count // across
    rim = -(-(conv_taps.shape[0] - 1) // 8) * 8
    dma, vmem = pltpu.SemaphoreType.DMA, pltpu.VMEM
    f32, bf16 = jnp.float32, jnp.bfloat16
    proj_rows = model_width // sp_count
    rows_total = sp_count * capacity
    shape = jax.ShapeDtypeStruct
    group = (across, capacity, width)
    return pl.pallas_call(
        functools.partial(fused_kernel, sp_count, tp_count),
        out_shape=(
            shape((tok_count, width), bf16),
            shape((tok_count, channels), bf16),
            shape((tok_count, channels), bf16),
            shape((proj_rows, channels), f32),
            shape((1, model_width, hidden), f32),
            shape((1, model_width, hidden), f32),
            shape((1, hidden, model_width), f32),
        ),
        in_specs=[pl.BlockSpec(memory_space=vmem)] + [pl.BlockSpec(memory_space=pl.ANY)] * 10,
        out_specs=[pl.BlockSpec(memory_space=vmem)] * 4 + [pl.BlockSpec(memory_space=pl.ANY)] * 3,
        scratch_shapes=[
            vmem((2, tok_count, model_width), bf16),
            vmem((model_width, 2 * hidden), bf16),
            vmem((hidden, model_width), bf16),
            vmem(conv_saved.shape, bf16),
            vmem(out_proj.shape, bf16),
            vmem(conv_taps.shape, f32),
            vmem(conv_saved.shape, bf16),
            vmem(conv_saved.shape, bf16),
            vmem((layers, 8, tok_count), f32),
            vmem((2, layers, tok_count, width), bf16),
            vmem((2, sp_count, capacity, model_width), bf16),
            vmem((across, capacity, tok_count), bf16),
            vmem((across, capacity, 128), f32),
            vmem((2, across - 1, chips, capacity, width), bf16),
            vmem((2, layers - 1, across - 1, capacity, width), bf16),
            vmem((tok_count, tok_count), bf16),
            vmem((rows_total, tok_count), bf16),
            vmem((tok_count, rows_total), bf16),
            vmem((hidden, rows_total), bf16),
            vmem((rows_total, 2 * hidden), bf16),
            vmem((sp_count, capacity, model_width), bf16),
            vmem((layers, chips) + group, bf16),
            vmem((layers, chips - 1) + group, bf16),
            vmem((layers, chips - 1) + group, bf16),
            vmem((layers,) + group, bf16),
            vmem((sp_count, capacity, width), bf16),
            vmem((tok_count, model_width), bf16),
            vmem((2, 8, 128), f32),
            vmem((2, tp_count, 8, 128), f32),
            vmem((sp_count, proj_rows, channels), bf16),
            vmem((sp_count, proj_rows, channels), bf16),
            vmem((rim, channels), f32),
            vmem((tok_count + rim, channels), f32),
            vmem((model_width, hidden), f32),
            vmem((model_width, hidden), f32),
            vmem((hidden, model_width), f32),
            dma((10,)),
            dma((3, model_width // 256)),
            dma((layers,)),
            dma((layers,)),
            dma((2, layers, 2)),
            dma((2, layers)),
        ]
        + [dma((2, layers, across - 1, chips))] * 2
        + [dma((2, layers, across, chips - 1))] * 2
        + [dma((2, layers, across, chips))] * 2
        + [dma((layers, chips))] * 2
        + [dma((layers, chips - 1))] * 2
        + [dma((layers, across)), dma((sp_count,))]
        + [dma((2, chips))] * 2
        + [dma((2, tp_count))] * 2
        + [dma((sp_count,))] * 2
        + [dma((1,))] * 2,
        compiler_params=pltpu.CompilerParams(
            collective_id=0, has_side_effects=True, vmem_limit_bytes=60 * 1024 * 1024
        ),
        name="fused",
    )(meta, stream, upstream, gate_w, up_w, down_w, *conv_args)


def on_device(
    upstream,
    stream,
    routes,
    route_weights,
    glu_value,
    glu_gate,
    conv_taps,
    conv_saved,
    out_proj,
    expert_gate,
    expert_up,
    expert_down,
):
    tok_count = upstream.shape[0]
    expert_count = lax.axis_size("sp")
    capacity = 4 * tok_count // expert_count
    meta = jnp.concatenate(
        [
            routes.T.astype(jnp.float32),
            route_weights.T,
            jnp.zeros((8 - 2 * routes.shape[1], tok_count), jnp.float32),
        ]
    )
    return fused(
        expert_count,
        lax.axis_size("tp"),
        capacity,
        meta,
        stream,
        upstream,
        expert_gate,
        expert_up,
        expert_down,
        conv_saved,
        out_proj,
        conv_taps,
        glu_value,
        glu_gate,
    )


def solution(mesh):
    in_specs = (
        P("sp", None),
        P("sp", None),
        P("sp", None),
        P("sp", None),
        P("sp", "tp"),
        P("sp", "tp"),
        P(None, "tp"),
        P("sp", "tp"),
        P(None, "tp"),
        P("sp", None, "tp"),
        P("sp", None, "tp"),
        P("sp", "tp", None),
    )
    out_specs = (
        P("sp", "tp"),
        P("sp", "tp"),
        P("sp", "tp"),
        P("sp", "tp"),
        P("sp", None, "tp"),
        P("sp", None, "tp"),
        P("sp", "tp", None),
    )
    return jax.shard_map(
        on_device, mesh=mesh, in_specs=in_specs, out_specs=out_specs, check_vma=False
    )
```

time: 182 us -> 153 us (0.84); the launches traced: 178 us -> 153 us
  matrix products: 35.9 us -> 0 us
  local copies, waits for them, and re-layouts: 8.8 us -> 16.8 us
  Pallas kernels: 131 us -> 133 us
    dot_general x11 -> x0, matrix products: 35.9 us -> none  [the longest x3 13.9 us: contract_rows(): lax.dot_general(left, right, (((0,), (0,)), ((), ())), preferred_element_...]
    unnamed x16 -> x11, local copies, waits for them, and re-layouts: 6.22 us -> 16.7 us
    pallas_call x2 -> x1, Pallas kernels: 131 us -> 133 us  [fused(): pl.pallas_call(functools.partial(fused_kernel, sp_count, tp_count), out_s...]
where the time goes in v1:
time: 153 us
  Pallas kernels  133 us (87%)
  local copies, waits for them, and re-layouts  16.8 us (11%)
  other arithmetic  2.03 us (1%)
    pallas_call x1, Pallas kernels, fused(): pl.pallas_call(functools.partial(fused_kernel, sp_count, tp_count), out_s...  133 us
    unnamed x11, local copies, waits for them, and re-layouts  16.7 us

profile of v1, /device:TPU:23, one launch (start us, length us, event | category | flops | bytes accessed | tf_op | source)
XLA Modules:
  0.0 152.5 jit_solution(12465744510895920404)
XLA Ops:
  0.6 0.1 pad.2.clone
  0.7 0.7 convert_bitcast_fusion
  1.4 1.3 maximum_maximum_fusion.meta_ref
  2.7 133.0 %fused.1 = (bf16[256,512]{1,0:T(8,128)(2,1)}, bf16[256,128]{1,0:T(8,128)(2,1)}, bf16[256,128]{1,0:T(8,128)(2,1)}, f32[256,128]{1,0:T(8,128)}, f32[1,2048,512]{2,...) custom-call(f32[8,256]{1,0:T(8,128)} %maximum_maximum_fusion.meta_ref, bf16[256,2048]{1,0:T(8,128)(2,1)} %stream_hbm.1, ...), custom_call_target="tpu_custom_call" | custom-call | tf_op jit(solution)/shard_map/fused/pallas_call | solution.py:751
  135.8 1.7 %copy.26 = bf16[256,512]{1,0:T(8,128)(2,1)} copy(bf16[256,512]{1,0:T(8,128)(2,1)} %get-tuple-element.14) | data formatting | bytes 524288
  137.5 1.5 copy.27
  138.9 1.5 copy.28
  140.4 1.6 %copy.29 = f32[256,128]{1,0:T(8,128)} copy(f32[256,128]{1,0:T(8,128)} %get-tuple-element.17) | data formatting | bytes 262144
  142.0 0.0 copy-start.1
  142.0 4.8 %copy.30 = f32[1,2048,512]{2,1,0:T(8,128)} copy(f32[1,2048,512]{2,1,0:T(8,128)} %get-tuple-element.18) | data formatting | bytes 8388608
  146.8 0.0 copy-done.1
  146.8 0.0 copy-start
  146.8 2.1 %copy.31 = f32[1,2048,512]{2,1,0:T(8,128)} copy(f32[1,2048,512]{2,1,0:T(8,128)S(1)} %copy-done.1) | data formatting | bytes 8388608
  148.9 1.6 %copy-done = f32[1,512,2048]{2,1,0:T(8,128)S(1)} copy-done((f32[1,512,2048]{2,1,0:T(8,128)S(1)}, f32[1,512,2048]{2,1,0:T(8,128)}, u32[]{:S(2)}) %copy-start) | copy-done | bytes 4194328
  150.5 2.0 %copy.32 = f32[1,512,2048]{2,1,0:T(8,128)} copy(f32[1,512,2048]{2,1,0:T(8,128)S(1)} %copy-done) | data formatting | bytes 8388608
  (1 shorter events, 0.0 us)
Async XLA Ops:
  142.0 4.8 %copy-start.1 = (f32[1,2048,512]{2,1,0:T(8,128)S(1)}, f32[1,2048,512]{2,1,0:T(8,128)}, u32[]{:S(2)}) copy-start(f32[1,2048,512]{2,1,0:T(8,128)} %get-tuple-element.19) | copy-start | bytes 12582916
  146.8 3.7 %copy-start = (f32[1,512,2048]{2,1,0:T(8,128)S(1)}, f32[1,512,2048]{2,1,0:T(8,128)}, u32[]{:S(2)}) copy-start(f32[1,512,2048]{2,1,0:T(8,128)} %get-tuple-element.20) | copy-start | bytes 12582916

commit v2 on v1

--- a/solution.py
+++ b/solution.py
@@ -63,7 +63,8 @@
 def fused_kernel(
     sp_count,
     tp_count,
-    meta_ref,
+    routes_ref,
+    route_weights_ref,
     stream_hbm,
     upstream_hbm,
     gate_hbm,
@@ -78,9 +79,9 @@
     grad_value_ref,
     grad_gate_ref,
     grad_proj_ref,
-    gate_out,
-    up_out,
-    down_out,
+    gate_acc,
+    up_acc,
+    down_acc,
     tokens,
     weights,
     down_ref,
@@ -89,8 +90,10 @@
     taps_ref,
     value_ref,
     gate_ref,
+    meta_ref,
     metas,
     chained,
+    extra,
     both,
     chosen,
     gains,
@@ -114,15 +117,13 @@
     parts_in,
     rim_in,
     padded,
-    gate_acc,
-    up_acc,
-    down_acc,
     load_sem,
-    store_sem,
     meta_send,
     meta_recv,
     chain_send,
     chain_recv,
+    extra_send,
+    extra_recv,
     cross_send,
     cross_recv,
     along_send,
@@ -176,6 +177,9 @@
     for load in loads:
         load.start()
 
+    meta_ref[...] = jnp.zeros(meta_ref.shape, f32)
+    meta_ref[0:2] = routes_ref[...].astype(f32)
+    meta_ref[2:4] = route_weights_ref[...]
     before[...] = jnp.where(
         lax.broadcasted_iota(jnp.int32, before.shape, 0)
         < lax.broadcasted_iota(jnp.int32, before.shape, 1),
@@ -255,15 +259,57 @@
         def _():
             own_chain(which, False).start()
 
+    last = layers - 1
+    far_side = jnp.where(layer > last - layer, 0, 1)
+    inside = (layer > 0) & (layer < last)
+
+    def column_at(hop):
+        return lax.rem(lane + tp_count - 2 * hop, tp_count)
+
+    def extra_copy(side, which, hop, own):
+        to = jnp.where(side == 0, me + across, me + sp_count - across)
+        here = extra.at[side, which, hop - 1]
+        return remote(
+            tokens.at[which, :, columns(column_at(hop))] if own else here,
+            here,
+            extra_send.at[side, which, hop - 1],
+            extra_recv.at[side, which, hop - 1],
+            sp=lax.rem(to, sp_count),
+        )
+
+    def all_extra():
+        return [(which, hop) for which in range(2) for hop in range(1, chips)]
+
+    for side, end in ((0, 0), (1, last)):
+
+        @pl.when(layer == end)
+        def _():
+            for which, hop in all_extra():
+                extra_copy(side, which, hop, True).start()
+
+    def stage_near():
+        @pl.when(inside)
+        def _():
+            for which, hop in all_extra():
+                extra_copy(1 - far_side, which, hop, False).wait_recv()
+                extra_copy(1 - far_side, which, hop, False).start()
+
+    def stage_far():
+        @pl.when(inside)
+        def _():
+            for which, hop in all_extra():
+                extra_copy(far_side, which, hop, False).wait_recv()
+                extra_copy(far_side, which, hop, False).start()
+
     def piece(which, block, column):
         return both.at[which, block, :, columns(column)]
 
-    def column_at(hop):
-        return lax.rem(lane + tp_count - 2 * hop, tp_count)
-
     def cross(which, step, index, hop):
         column = column_at(hop)
-        source = near_out.at[which, index - 1, hop] if step == 0 else cross_out.at[which, step - 1, index - 1]
+        if step in (0, last):
+            source = near_out.at[min(step, 1), which, index - 1, hop]
+        else:
+            source = cross_out.at[which, step - 1, index - 1]
         return remote(
             source,
             piece(which, block_at(step, 0), column),
@@ -327,7 +373,7 @@
             for which in range(2):
                 for index in range(1, across):
                     for hop in range(chips):
-                        near_out[which, index - 1, hop] = picked(
+                        near_out[0, which, index - 1, hop] = picked(
                             which, index, tokens[which, :, columns(column_at(hop))]
                         )
                         begin(cross(which, 0, index, hop))
@@ -349,25 +395,44 @@
                 chain_on(which, step).wait_recv()
 
             for index in range(1, across):
-                cross_out[which, step - 1, index - 1] = picked(which, index, chained[which, source])
+                rows = picked(which, index, chained[which, source])
+                if step == last:
+                    near_out[1, which, index - 1, 0] = rows
+                else:
+                    cross_out[which, step - 1, index - 1] = rows
                 begin(cross(which, step, index, 0))
             both[which, block_at(step, 0), :, columns(lane)] = picked(which, 0, chained[which, source])
-            for hop in range(1, chips):
-                begin(along(which, step, 0, hop))
+            if step < last:
+                for hop in range(1, chips):
+                    begin(along(which, step, 0, hop))
             begin(twin(which, step, 0, 0))
+
+    def stage_extra():
+        for which, hop in all_extra():
+
+            @pl.when(jnp.logical_not(inside))
+            def _():
+                extra_copy(far_side, which, hop, False).wait_recv()
+
+            source = extra[far_side, which, hop - 1]
+            for index in range(1, across):
+                near_out[1, which, index - 1, hop] = picked(which, index, source)
+                begin(cross(which, last, index, hop))
+            both[which, block_at(last, 0), :, columns(column_at(hop))] = picked(which, 0, source)
+            begin(twin(which, last, 0, hop))
 
     def stage_cross(step):
         for which in range(2):
             for index in range(1, across):
-                for hop in range(chips if step == 0 else 1):
+                for hop in range(chips if step in (0, last) else 1):
                     cross(which, step, index, hop).wait_recv()
-                    if step:
+                    if step not in (0, last):
                         for side in range(1, chips):
                             begin(along(which, step, index, side))
                     begin(twin(which, step, index, hop))
 
     def stage_along(step):
-        if step == 0:
+        if step in (0, last):
             return
         for which in range(2):
             for index in range(across):
@@ -540,48 +605,45 @@
         picks_all[expert * capacity : (expert + 1) * capacity] = pick.astype(bf16)
     picks_t[...] = picks_all[...].astype(f32).T.astype(bf16)
 
-    if layers > 1:
-        stage_forward(1)
-        stage_select(1)
-    if layers > 2:
-        stage_forward(2)
+    stage_forward(1)
+    stage_select(1)
+    for step in range(2, min(3, layers)):
+        stage_forward(step)
     stage_cross(0)
     stage_expert(0)
     stage_pair(0)
-    for step in range(2, layers + 1):
-        stage_cross(step - 1)
-        if step < layers:
-            stage_select(step)
+    for step in range(2, layers):
+        if step == 2:
+            stage_cross(1)
+        stage_select(step)
+        if step == 2:
+            stage_near()
         if step + 1 < layers:
             stage_forward(step + 1)
         stage_along(step - 1)
+        if step < last:
+            stage_cross(step)
+        if step == last:
+            stage_far()
         stage_expert(step - 1)
         stage_return(step - 2)
         stage_pair(step - 1)
+    stage_extra()
+    stage_cross(last)
+    stage_expert(last)
+    stage_return(last - 1)
+    stage_pair(last)
 
     tile_width = 256
     tiles = model_width // tile_width
     rows_total = sp_count * capacity
 
-    def down_store(tile):
-        at = pl.ds(pl.multiple_of(tile * tile_width, tile_width), tile_width)
-        return pltpu.make_async_copy(down_acc.at[:, at], down_out.at[0, :, at], store_sem.at[0, tile])
-
-    def gate_store(tile):
-        at = pl.ds(pl.multiple_of(tile * tile_width, tile_width), tile_width)
-        return pltpu.make_async_copy(gate_acc.at[at], gate_out.at[0, at], store_sem.at[1, tile])
-
-    def up_store(tile):
-        at = pl.ds(pl.multiple_of(tile * tile_width, tile_width), tile_width)
-        return pltpu.make_async_copy(up_acc.at[at], up_out.at[0, at], store_sem.at[2, tile])
-
     @pl.loop(0, tiles)
     def _(tile):
         at = pl.ds(pl.multiple_of(tile * tile_width, tile_width), tile_width)
-        down_acc[:, at] = jnp.dot(
+        down_acc[0, :, at] = jnp.dot(
             act_t[...], both[1, :, :, at].reshape(rows_total, tile_width), preferred_element_type=f32
         )
-        down_store(tile).start()
 
     stage_return(layers - 1)
 
@@ -589,10 +651,8 @@
     def _(tile):
         at = pl.ds(pl.multiple_of(tile * tile_width, tile_width), tile_width)
         left = both[0, :, :, at].reshape(rows_total, tile_width)
-        gate_acc[at] = contract_rows(left, slopes[:, :hidden])
-        up_acc[at] = contract_rows(left, slopes[:, hidden:])
-        gate_store(tile).start()
-        up_store(tile).start()
+        gate_acc[0, at] = contract_rows(left, slopes[:, :hidden])
+        up_acc[0, at] = contract_rows(left, slopes[:, hidden:])
 
     total_sum, square_sum = shared(0)
     mean_c = total_sum / conv_width
@@ -706,15 +766,21 @@
         give_parts(step).wait_recv()
         summed += parts_in[step].astype(f32)
     grad_proj_ref[...] = summed
-
-    @pl.loop(0, tiles)
-    def _(tile):
-        down_store(tile).wait()
-        gate_store(tile).wait()
-        up_store(tile).wait()
-
     for copy in started:
         copy.wait_send()
+    for side, end in ((0, 0), (1, last)):
+
+        @pl.when(layer == end)
+        def _():
+            for which, hop in all_extra():
+                extra_copy(side, which, hop, True).wait_send()
+
+    @pl.when(inside)
+    def _():
+        for side in range(2):
+            for which, hop in all_extra():
+                extra_copy(side, which, hop, False).wait_send()
+
     for which in range(2):
 
         @pl.when(layer < layers - 1)
@@ -732,7 +798,9 @@
                 chain_on(which, step).wait_send()
 
 
-def fused(sp_count, tp_count, capacity, meta, stream, upstream, gate_w, up_w, down_w, *conv_args):
+def fused(
+    sp_count, tp_count, capacity, routes, gains, stream, upstream, gate_w, up_w, down_w, *conv_args
+):
     conv_saved, out_proj, conv_taps = conv_args[:3]
     tok_count, model_width = stream.shape
     channels = conv_saved.shape[1]
@@ -746,7 +814,7 @@
     f32, bf16 = jnp.float32, jnp.bfloat16
     proj_rows = model_width // sp_count
     rows_total = sp_count * capacity
-    shape = jax.ShapeDtypeStruct
+    shape = pltpu.VMEM
     group = (across, capacity, width)
     return pl.pallas_call(
         functools.partial(fused_kernel, sp_count, tp_count),
@@ -759,8 +827,8 @@
             shape((1, model_width, hidden), f32),
             shape((1, hidden, model_width), f32),
         ),
-        in_specs=[pl.BlockSpec(memory_space=vmem)] + [pl.BlockSpec(memory_space=pl.ANY)] * 10,
-        out_specs=[pl.BlockSpec(memory_space=vmem)] * 4 + [pl.BlockSpec(memory_space=pl.ANY)] * 3,
+        in_specs=[pl.BlockSpec(memory_space=vmem)] * 2 + [pl.BlockSpec(memory_space=pl.ANY)] * 10,
+        out_specs=[pl.BlockSpec(memory_space=vmem)] * 7,
         scratch_shapes=[
             vmem((2, tok_count, model_width), bf16),
             vmem((model_width, 2 * hidden), bf16),
@@ -770,13 +838,15 @@
             vmem(conv_taps.shape, f32),
             vmem(conv_saved.shape, bf16),
             vmem(conv_saved.shape, bf16),
+            vmem((8, tok_count), f32),
             vmem((layers, 8, tok_count), f32),
             vmem((2, layers, tok_count, width), bf16),
+            vmem((2, 2, chips - 1, tok_count, width), bf16),
             vmem((2, sp_count, capacity, model_width), bf16),
             vmem((across, capacity, tok_count), bf16),
             vmem((across, capacity, 128), f32),
-            vmem((2, across - 1, chips, capacity, width), bf16),
-            vmem((2, layers - 1, across - 1, capacity, width), bf16),
+            vmem((2, 2, across - 1, chips, capacity, width), bf16),
+            vmem((2, layers - 2, across - 1, capacity, width), bf16),
             vmem((tok_count, tok_count), bf16),
             vmem((rows_total, tok_count), bf16),
             vmem((tok_count, rows_total), bf16),
@@ -795,15 +865,13 @@
             vmem((sp_count, proj_rows, channels), bf16),
             vmem((rim, channels), f32),
             vmem((tok_count + rim, channels), f32),
-            vmem((model_width, hidden), f32),
-            vmem((model_width, hidden), f32),
-            vmem((hidden, model_width), f32),
             dma((10,)),
-            dma((3, model_width // 256)),
             dma((layers,)),
             dma((layers,)),
             dma((2, layers, 2)),
             dma((2, layers)),
+            dma((2, 2, chips - 1)),
+            dma((2, 2, chips - 1)),
         ]
         + [dma((2, layers, across - 1, chips))] * 2
         + [dma((2, layers, across, chips - 1))] * 2
@@ -816,10 +884,34 @@
         + [dma((sp_count,))] * 2
         + [dma((1,))] * 2,
         compiler_params=pltpu.CompilerParams(
-            collective_id=0, has_side_effects=True, vmem_limit_bytes=60 * 1024 * 1024
+            collective_id=0, has_side_effects=True, vmem_limit_bytes=46 * 1024 * 1024
         ),
         name="fused",
-    )(meta, stream, upstream, gate_w, up_w, down_w, *conv_args)
+    )(routes, gains, stream, upstream, gate_w, up_w, down_w, *conv_args)
+
+
+def emit_kernel(*refs):
+    count = len(refs) // 2
+    copies = [
+        pltpu.make_async_copy(refs[at], refs[count + at], refs[-1].at[at]) for at in range(count)
+    ]
+    for copy in reversed(copies):
+        copy.start()
+    for copy in copies:
+        copy.wait()
+
+
+def emit(results):
+    count = len(results)
+    return pl.pallas_call(
+        emit_kernel,
+        out_shape=tuple(jax.ShapeDtypeStruct(item.shape, item.dtype) for item in results),
+        in_specs=[pl.BlockSpec(memory_space=pltpu.VMEM)] * count,
+        out_specs=[pl.BlockSpec(memory_space=pl.ANY)] * count,
+        scratch_shapes=[pltpu.SemaphoreType.DMA((count,))],
+        compiler_params=pltpu.CompilerParams(vmem_limit_bytes=1024 * 1024),
+        name="emit",
+    )(*[pltpu.with_memory_space_constraint(item, pltpu.VMEM) for item in results])
 
 
 def on_device(
@@ -839,18 +931,12 @@
     tok_count = upstream.shape[0]
     expert_count = lax.axis_size("sp")
     capacity = 4 * tok_count // expert_count
-    meta = jnp.concatenate(
-        [
-            routes.T.astype(jnp.float32),
-            route_weights.T,
-            jnp.zeros((8 - 2 * routes.shape[1], tok_count), jnp.float32),
-        ]
-    )
-    return fused(
+    results = fused(
         expert_count,
         lax.axis_size("tp"),
         capacity,
-        meta,
+        routes.T,
+        route_weights.T,
         stream,
         upstream,
         expert_gate,
@@ -862,6 +948,7 @@
         glu_value,
         glu_gate,
     )
+    return emit(results)
 
 
 def solution(mesh):

time: 153 us -> 129 us (0.84)
  local copies, waits for them, and re-layouts: 16.8 us -> 0 us
  Pallas kernels: 133 us -> 128 us
  other arithmetic: 2.03 us -> 0 us
    unnamed x11 -> x0, local copies, waits for them, and re-layouts: 16.7 us -> none
    pallas_call x1, Pallas kernels: 133 us -> 123 us  [fused(): pl.pallas_call(functools.partial(fused_kernel, sp_count, tp_count), out_s...]
    pallas_call x0 -> x1, Pallas kernels: none -> 4.76 us  [emit(): pl.pallas_call(emit_kernel, out_shape=tuple((jax.ShapeDtypeStruct(item.sh...]
where the time goes in v2:
time: 129 us
  Pallas kernels  128 us (99%)
    pallas_call x1, Pallas kernels, fused(): pl.pallas_call(functools.partial(fused_kernel, sp_count, tp_count), out_s...  123 us
    pallas_call x1, Pallas kernels, emit(): pl.pallas_call(emit_kernel, out_shape=tuple((jax.ShapeDtypeStruct(item.sh...  4.76 us

profile of v2, /device:TPU:23, one launch (start us, length us, event | category | flops | bytes accessed | tf_op | source)
XLA Modules:
  0.0 128.7 jit_solution(13576312574103820012)
XLA Ops:
  0.6 123.3 %fused.1 = (bf16[256,512]{1,0:T(8,128)(2,1)S(1)}, bf16[256,128]{1,0:T(8,128)(2,1)S(1)}, bf16[256,128]{1,0:T(8,128)(2,1)S(1)}, f32[256,128]{1,0:T(8,128)S(1)}, f3...) custom-call(s32[2,256]{1,0:T(2,128)} %bitcast.2, f32[2,256]{1,0:T(2,128)} %bitcast.3, ...), custom_call_target="tpu_custom_call" | custom-call | tf_op jit(solution)/shard_map/fused/pallas_call | solution.py:819
  123.9 4.8 %emit.1 = (bf16[256,512]{1,0:T(8,128)(2,1)}, bf16[256,128]{1,0:T(8,128)(2,1)}, bf16[256,128]{1,0:T(8,128)(2,1)}, f32[256,128]{1,0:T(8,128)}, f32[1,2048,512]{2,1...) custom-call(bf16[256,512]{1,0:T(8,128)(2,1)S(1)} %get-tuple-element.14.refs_0_, ...), custom_call_target="tpu_custom_call" | custom-call | tf_op jit(solution)/shard_map/emit/pallas_call | solution.py:906

commit v3 on v2

--- a/solution.py
+++ b/solution.py
@@ -294,13 +294,6 @@
                 extra_copy(1 - far_side, which, hop, False).wait_recv()
                 extra_copy(1 - far_side, which, hop, False).start()
 
-    def stage_far():
-        @pl.when(inside)
-        def _():
-            for which, hop in all_extra():
-                extra_copy(far_side, which, hop, False).wait_recv()
-                extra_copy(far_side, which, hop, False).start()
-
     def piece(which, block, column):
         return both.at[which, block, :, columns(column)]
 
@@ -323,8 +316,8 @@
         return remote(
             here,
             here,
-            along_send.at[which, step, index, hop - 1],
-            along_recv.at[which, step, index, hop - 1],
+            along_send.at[which, step - 1, index, hop - 1],
+            along_recv.at[which, step - 1, index, hop - 1],
             tp=lax.rem(lane + 2 * hop, tp_count),
         )
 
@@ -396,30 +389,62 @@
 
             for index in range(1, across):
                 rows = picked(which, index, chained[which, source])
-                if step == last:
-                    near_out[1, which, index - 1, 0] = rows
-                else:
-                    cross_out[which, step - 1, index - 1] = rows
+                cross_out[which, step - 1, index - 1] = rows
                 begin(cross(which, step, index, 0))
             both[which, block_at(step, 0), :, columns(lane)] = picked(which, 0, chained[which, source])
-            if step < last:
-                for hop in range(1, chips):
-                    begin(along(which, step, 0, hop))
+            for hop in range(1, chips):
+                begin(along(which, step, 0, hop))
             begin(twin(which, step, 0, 0))
 
+    def send_last(which, hop, source):
+        for index in range(1, across):
+            near_out[1, which, index - 1, hop] = picked(which, index, source)
+            cross(which, last, index, hop).start()
+        both[which, block_at(last, 0), :, columns(column_at(hop))] = picked(which, 0, source)
+        twin(which, last, 0, hop).start()
+
+    def select_last(wait):
+        source = at_layer[last]
+        remote(
+            meta_ref, metas.at[source], meta_send.at[0], meta_recv.at[source], sp=lax.rem(me + across, sp_count)
+        ).wait_recv()
+        choose(metas[source])
+        for which in range(2):
+            if wait:
+                chain_on(which, last).wait_recv()
+            send_last(which, 0, chained[which, source])
+
+    def stage_inner():
+        @pl.when(inside)
+        def _():
+            select_last(False)
+
+    def stage_outer():
+        @pl.when(jnp.logical_not(inside))
+        def _():
+            select_last(True)
+
+    def stage_far():
+        @pl.when(inside)
+        def _():
+            for which, hop in all_extra():
+                extra_copy(far_side, which, hop, False).wait_recv()
+                extra_copy(far_side, which, hop, False).start()
+            for which, hop in all_extra():
+                send_last(which, hop, extra[far_side, which, hop - 1])
+
     def stage_extra():
-        for which, hop in all_extra():
-
-            @pl.when(jnp.logical_not(inside))
-            def _():
+        @pl.when(jnp.logical_not(inside))
+        def _():
+            for which, hop in all_extra():
                 extra_copy(far_side, which, hop, False).wait_recv()
-
-            source = extra[far_side, which, hop - 1]
-            for index in range(1, across):
-                near_out[1, which, index - 1, hop] = picked(which, index, source)
-                begin(cross(which, last, index, hop))
-            both[which, block_at(last, 0), :, columns(column_at(hop))] = picked(which, 0, source)
-            begin(twin(which, last, 0, hop))
+                send_last(which, hop, extra[far_side, which, hop - 1])
+
+        for which in range(2):
+            for hop in range(chips):
+                started.append(twin(which, last, 0, hop))
+                for index in range(1, across):
+                    started.append(cross(which, last, index, hop))
 
     def stage_cross(step):
         for which in range(2):
@@ -440,29 +465,42 @@
                     along(which, step, index, hop).wait_recv()
                     begin(twin(which, step, index, hop))
 
-    def group_at(step):
-        return pl.ds(at_layer[step] * across, across)
+    split_last = capacity % 128 == 0
+
+    def blocks_of(step, index):
+        if index is None:
+            return at_layer[step] * across, across
+        return block_at(step, index), 1
+
+    def group_at(step, index):
+        first, count = blocks_of(step, index)
+        return pl.ds(first, count)
+
+    def slot_of(step, index):
+        return step + (index or 0)
 
     hidden_tile = min(hidden, 256)
 
-    def stage_expert(step):
+    def stage_expert(step, part=None):
         for which in range(2):
-            for index in range(across):
+            for index in range(across) if part is None else [part]:
                 if step or index:
                     for hop in range(chips):
                         twin(which, step, index, hop).wait_recv()
         if step == 0:
             for load in loads[3:6]:
                 load.wait()
-        first = pl.multiple_of(at_layer[step] * group_rows, group_rows)
-        rows_at = pl.ds(first, group_rows)
+        first, count = blocks_of(step, part)
+        size = count * capacity
+        rows_at = pl.ds(pl.multiple_of(first * capacity, size), size)
+        group = group_at(step, part)
 
         @pl.loop(0, hidden // hidden_tile)
         def _(tile):
             units = pl.ds(pl.multiple_of(tile * hidden_tile, hidden_tile), hidden_tile)
             up_units = pl.ds(pl.multiple_of(hidden + tile * hidden_tile, hidden_tile), hidden_tile)
-            rows = both[0, group_at(step)].reshape(group_rows, model_width)
-            cot = both[1, group_at(step)].reshape(group_rows, model_width)
+            rows = both[0, group].reshape(size, model_width)
+            cot = both[1, group].reshape(size, model_width)
             gate_pre = jnp.dot(rows, weights[:, units], preferred_element_type=f32)
             up_pre = jnp.dot(rows, weights[:, up_units], preferred_element_type=f32)
             grad_act = times_transposed(cot, down_ref[units, :])
@@ -482,61 +520,66 @@
         @pl.loop(0, tp_count)
         def _(tile):
             value = times_transposed(slopes[rows_at, :], weights[columns(tile), :])
-            partial[group_at(step), :, columns(tile)] = value.astype(bf16).reshape(
-                across, capacity, width
-            )
+            partial[group, :, columns(tile)] = value.astype(bf16).reshape(count, capacity, width)
 
         for hop in list(range(1, chips)) + [0]:
-            begin(swapped(step, hop))
-
-    def swapped(step, hop):
+            begin(swapped(step, hop, part))
+
+    def swapped(step, hop, part):
         other = lax.rem(lane + 2 * hop, tp_count) + 1 - 2 * core
-        return remote(
-            partial.at[group_at(step), :, columns(other)],
-            pair_in.at[step, hop],
-            pair_send.at[step, hop],
-            pair_recv.at[step, hop],
+        slot, count = slot_of(step, part), blocks_of(step, part)[1]
+        return remote(
+            partial.at[group_at(step, part), :, columns(other)],
+            pair_in.at[slot, hop, pl.ds(0, count)],
+            pair_send.at[slot, hop],
+            pair_recv.at[slot, hop],
             tp=partner,
         )
 
-    def beside(step, hop):
-        return remote(
-            side_out.at[step, hop - 1],
-            side_in.at[step, hop - 1],
-            side_send.at[step, hop - 1],
-            side_recv.at[step, hop - 1],
+    def beside(step, hop, part):
+        slot, count = slot_of(step, part), blocks_of(step, part)[1]
+        return remote(
+            side_out.at[slot, hop - 1, pl.ds(0, count)],
+            side_in.at[slot, hop - 1, pl.ds(0, count)],
+            side_send.at[slot, hop - 1],
+            side_recv.at[slot, hop - 1],
             tp=lax.rem(lane + 2 * hop, tp_count),
         )
 
-    def pair_sum(step, hop):
+    def pair_sum(step, hop, part):
         column = lax.rem(lane + 2 * hop, tp_count)
-        return partial[group_at(step), :, columns(column)].astype(f32) + pair_in[step, hop].astype(f32)
-
-    def stage_pair(step):
+        slot, count = slot_of(step, part), blocks_of(step, part)[1]
+        mine = partial[group_at(step, part), :, columns(column)].astype(f32)
+        return mine + pair_in[slot, hop, pl.ds(0, count)].astype(f32)
+
+    def stage_pair(step, part=None):
+        slot, count = slot_of(step, part), blocks_of(step, part)[1]
         for hop in range(1, chips):
-            swapped(step, hop).wait_recv()
-            side_out[step, hop - 1] = pair_sum(step, hop).astype(bf16)
-            begin(beside(step, hop))
-
-    def stage_return(step):
-        swapped(step, 0).wait_recv()
-        value = pair_sum(step, 0)
+            swapped(step, hop, part).wait_recv()
+            side_out[slot, hop - 1, pl.ds(0, count)] = pair_sum(step, hop, part).astype(bf16)
+            begin(beside(step, hop, part))
+
+    def stage_return(step, part=None):
+        slot, count = slot_of(step, part), blocks_of(step, part)[1]
+        swapped(step, 0, part).wait_recv()
+        value = pair_sum(step, 0, part)
         for hop in range(1, chips):
-            beside(step, hop).wait_recv()
-            value += side_in[step, hop - 1].astype(f32)
-        total[step] = value.astype(bf16)
-        for index in range(across):
-            spot = lax.rem(place + index, across)
+            beside(step, hop, part).wait_recv()
+            value += side_in[slot, hop - 1, pl.ds(0, count)].astype(f32)
+        total[slot, pl.ds(0, count)] = value.astype(bf16)
+        for index in range(across) if part is None else [part]:
+            block = block_at(step, index)
+            spot = lax.rem(place + across - index, across) if part is None else 0
             if step == 0 and index == 0:
                 returned[me] = total[0, spot]
             else:
                 begin(
                     remote(
-                        total.at[step, spot],
+                        total.at[slot, spot],
                         returned.at[me],
                         far_send.at[step, index],
                         far_recv.at[me],
-                        sp=at_layer[step] * across + spot,
+                        sp=block,
                     )
                 )
 
@@ -551,8 +594,8 @@
         return remote(
             stat_out.at[phase],
             stat_in.at[phase, hop],
-            stat_send.at[phase, hop],
-            stat_recv.at[phase, hop],
+            stat_send.at[phase, hop - 1],
+            stat_recv.at[phase, hop - 1],
             tp=lax.rem(lane + hop, tp_count),
         )
 
@@ -615,24 +658,42 @@
     for step in range(2, layers):
         if step == 2:
             stage_cross(1)
-        stage_select(step)
+        if step < last:
+            stage_select(step)
+        else:
+            stage_outer()
         if step == 2:
             stage_near()
         if step + 1 < layers:
             stage_forward(step + 1)
+        if step == last - 1:
+            stage_inner()
         stage_along(step - 1)
         if step < last:
             stage_cross(step)
+        if step == last - 1:
+            stage_far()
+        if step < last:
+            stage_return(step - 2)
+        stage_expert(step - 1)
         if step == last:
-            stage_far()
-        stage_expert(step - 1)
-        stage_return(step - 2)
+            stage_extra()
+            stage_return(step - 2)
         stage_pair(step - 1)
-    stage_extra()
-    stage_cross(last)
-    stage_expert(last)
-    stage_return(last - 1)
-    stage_pair(last)
+    if split_last:
+        stage_expert(last, 0)
+        stage_pair(last, 0)
+        stage_cross(last)
+        stage_return(last - 1)
+        for index in range(1, across):
+            stage_expert(last, index)
+            stage_return(last, index - 1)
+            stage_pair(last, index)
+    else:
+        stage_cross(last)
+        stage_expert(last)
+        stage_return(last - 1)
+        stage_pair(last)
 
     tile_width = 256
     tiles = model_width // tile_width
@@ -645,14 +706,15 @@
             act_t[...], both[1, :, :, at].reshape(rows_total, tile_width), preferred_element_type=f32
         )
 
-    stage_return(layers - 1)
-
-    @pl.loop(0, tiles)
-    def _(tile):
+    def gate_up_tile(tile):
         at = pl.ds(pl.multiple_of(tile * tile_width, tile_width), tile_width)
         left = both[0, :, :, at].reshape(rows_total, tile_width)
         gate_acc[0, at] = contract_rows(left, slopes[:, :hidden])
         up_acc[0, at] = contract_rows(left, slopes[:, hidden:])
+
+    pl.loop(0, tiles // 4)(gate_up_tile)
+    stage_return(last, across - 1 if split_last else None)
+    pl.loop(tiles // 4, tiles)(gate_up_tile)
 
     total_sum, square_sum = shared(0)
     mean_c = total_sum / conv_width
@@ -809,6 +871,7 @@
     chips = tp_count // 2
     across = chips
     layers = sp_count // across
+    slots = layers + across - 1
     rim = -(-(conv_taps.shape[0] - 1) // 8) * 8
     dma, vmem = pltpu.SemaphoreType.DMA, pltpu.VMEM
     f32, bf16 = jnp.float32, jnp.bfloat16
@@ -853,10 +916,10 @@
             vmem((hidden, rows_total), bf16),
             vmem((rows_total, 2 * hidden), bf16),
             vmem((sp_count, capacity, model_width), bf16),
-            vmem((layers, chips) + group, bf16),
-            vmem((layers, chips - 1) + group, bf16),
-            vmem((layers, chips - 1) + group, bf16),
-            vmem((layers,) + group, bf16),
+            vmem((slots, chips) + group, bf16),
+            vmem((slots, chips - 1) + group, bf16),
+            vmem((slots, chips - 1) + group, bf16),
+            vmem((slots,) + group, bf16),
             vmem((sp_count, capacity, width), bf16),
             vmem((tok_count, model_width), bf16),
             vmem((2, 8, 128), f32),
@@ -874,17 +937,17 @@
             dma((2, 2, chips - 1)),
         ]
         + [dma((2, layers, across - 1, chips))] * 2
-        + [dma((2, layers, across, chips - 1))] * 2
+        + [dma((2, layers - 2, across, chips - 1))] * 2
         + [dma((2, layers, across, chips))] * 2
-        + [dma((layers, chips))] * 2
-        + [dma((layers, chips - 1))] * 2
+        + [dma((slots, chips))] * 2
+        + [dma((slots, chips - 1))] * 2
         + [dma((layers, across)), dma((sp_count,))]
         + [dma((2, chips))] * 2
-        + [dma((2, tp_count))] * 2
+        + [dma((2, tp_count - 1))] * 2
         + [dma((sp_count,))] * 2
         + [dma((1,))] * 2,
         compiler_params=pltpu.CompilerParams(
-            collective_id=0, has_side_effects=True, vmem_limit_bytes=46 * 1024 * 1024
+            collective_id=0, has_side_effects=True, vmem_limit_bytes=47 * 1024 * 1024
         ),
         name="fused",
     )(routes, gains, stream, upstream, gate_w, up_w, down_w, *conv_args)

time: 129 us -> 114 us (0.88)
  Pallas kernels: 128 us -> 113 us
    pallas_call x1, Pallas kernels: 123 us -> 108 us  [fused(): pl.pallas_call(functools.partial(fused_kernel, sp_count, tp_count), out_s...]
where the time goes in v3:
time: 114 us; the launch traced here: 113 us
  Pallas kernels  113 us (99%)
    pallas_call x1, Pallas kernels, fused(): pl.pallas_call(functools.partial(fused_kernel, sp_count, tp_count), out_s...  108 us
    pallas_call x1, Pallas kernels, emit(): pl.pallas_call(emit_kernel, out_shape=tuple((jax.ShapeDtypeStruct(item.sh...  4.76 us

profile of v3, /device:TPU:23, one launch (start us, length us, event | category | flops | bytes accessed | tf_op | source)
XLA Modules:
  0.0 113.5 jit_solution(4053972632527055692)
XLA Ops:
  0.6 107.9 %fused.1 = (bf16[256,512]{1,0:T(8,128)(2,1)S(1)}, bf16[256,128]{1,0:T(8,128)(2,1)S(1)}, bf16[256,128]{1,0:T(8,128)(2,1)S(1)}, f32[256,128]{1,0:T(8,128)S(1)}, f3...) custom-call(s32[2,256]{1,0:T(2,128)} %bitcast.2, f32[2,256]{1,0:T(2,128)} %bitcast.3, ...), custom_call_target="tpu_custom_call" | custom-call | tf_op jit(solution)/shard_map/fused/pallas_call | solution.py:882
  108.5 4.8 %emit.1 = (bf16[256,512]{1,0:T(8,128)(2,1)}, bf16[256,128]{1,0:T(8,128)(2,1)}, bf16[256,128]{1,0:T(8,128)(2,1)}, f32[256,128]{1,0:T(8,128)}, f32[1,2048,512]{2,1...) custom-call(bf16[256,512]{1,0:T(8,128)(2,1)S(1)} %get-tuple-element.14.refs_0_, ...), custom_call_target="tpu_custom_call" | custom-call | tf_op jit(solution)/shard_map/emit/pallas_call | solution.py:969

commit v4 on v3

--- a/solution.py
+++ b/solution.py
@@ -203,7 +203,8 @@
         inner = jnp.minimum(layer, layers - 1 - layer)
         paired = step <= 2 * inner
         reach = jnp.where(paired, (step + 1) // 2, step - inner)
-        below = jnp.where(paired, step % 2 == 1, layer > layers - 1 - layer)
+        upper = layer > layers - 1 - layer
+        below = jnp.where(paired, jnp.logical_xor(upper, step % 2 == 0), upper)
         return jnp.where(below, layer - reach, layer + reach)
 
     at_layer = [layer_at(step) for step in range(layers)]
@@ -306,7 +307,7 @@
         return remote(
             source,
             piece(which, block_at(step, 0), column),
-            cross_send.at[which, step, index - 1, hop],
+            cross_send.at[0 if step in (0, last) else 1],
             cross_recv.at[which, step, index - 1, hop],
             sp=layer * across + lax.rem(place + index, across),
         )
@@ -316,7 +317,7 @@
         return remote(
             here,
             here,
-            along_send.at[which, step - 1, index, hop - 1],
+            along_send.at[0],
             along_recv.at[which, step - 1, index, hop - 1],
             tp=lax.rem(lane + 2 * hop, tp_count),
         )
@@ -326,7 +327,7 @@
         return remote(
             here,
             here,
-            twin_send.at[which, step, index, hop],
+            twin_send.at[0],
             twin_recv.at[which, step, index, hop],
             tp=partner,
         )
@@ -369,7 +370,7 @@
                         near_out[0, which, index - 1, hop] = picked(
                             which, index, tokens[which, :, columns(column_at(hop))]
                         )
-                        begin(cross(which, 0, index, hop))
+                        cross(which, 0, index, hop).start()
             for which in range(2):
                 for column in range(tp_count):
                     both[which, me, :, column * width : (column + 1) * width] = picked(
@@ -390,11 +391,11 @@
             for index in range(1, across):
                 rows = picked(which, index, chained[which, source])
                 cross_out[which, step - 1, index - 1] = rows
-                begin(cross(which, step, index, 0))
+                cross(which, step, index, 0).start()
             both[which, block_at(step, 0), :, columns(lane)] = picked(which, 0, chained[which, source])
             for hop in range(1, chips):
-                begin(along(which, step, 0, hop))
-            begin(twin(which, step, 0, 0))
+                along(which, step, 0, hop).start()
+            twin(which, step, 0, 0).start()
 
     def send_last(which, hop, source):
         for index in range(1, across):
@@ -440,12 +441,6 @@
                 extra_copy(far_side, which, hop, False).wait_recv()
                 send_last(which, hop, extra[far_side, which, hop - 1])
 
-        for which in range(2):
-            for hop in range(chips):
-                started.append(twin(which, last, 0, hop))
-                for index in range(1, across):
-                    started.append(cross(which, last, index, hop))
-
     def stage_cross(step):
         for which in range(2):
             for index in range(1, across):
@@ -453,8 +448,8 @@
                     cross(which, step, index, hop).wait_recv()
                     if step not in (0, last):
                         for side in range(1, chips):
-                            begin(along(which, step, index, side))
-                    begin(twin(which, step, index, hop))
+                            along(which, step, index, side).start()
+                    twin(which, step, index, hop).start()
 
     def stage_along(step):
         if step in (0, last):
@@ -463,7 +458,7 @@
             for index in range(across):
                 for hop in range(1, chips):
                     along(which, step, index, hop).wait_recv()
-                    begin(twin(which, step, index, hop))
+                    twin(which, step, index, hop).start()
 
     split_last = capacity % 128 == 0
 
@@ -523,7 +518,7 @@
             partial[group, :, columns(tile)] = value.astype(bf16).reshape(count, capacity, width)
 
         for hop in list(range(1, chips)) + [0]:
-            begin(swapped(step, hop, part))
+            swapped(step, hop, part).start()
 
     def swapped(step, hop, part):
         other = lax.rem(lane + 2 * hop, tp_count) + 1 - 2 * core
@@ -531,7 +526,7 @@
         return remote(
             partial.at[group_at(step, part), :, columns(other)],
             pair_in.at[slot, hop, pl.ds(0, count)],
-            pair_send.at[slot, hop],
+            pair_send.at[0],
             pair_recv.at[slot, hop],
             tp=partner,
         )
@@ -541,7 +536,7 @@
         return remote(
             side_out.at[slot, hop - 1, pl.ds(0, count)],
             side_in.at[slot, hop - 1, pl.ds(0, count)],
-            side_send.at[slot, hop - 1],
+            side_send.at[0],
             side_recv.at[slot, hop - 1],
             tp=lax.rem(lane + 2 * hop, tp_count),
         )
@@ -557,7 +552,7 @@
         for hop in range(1, chips):
             swapped(step, hop, part).wait_recv()
             side_out[slot, hop - 1, pl.ds(0, count)] = pair_sum(step, hop, part).astype(bf16)
-            begin(beside(step, hop, part))
+            beside(step, hop, part).start()
 
     def stage_return(step, part=None):
         slot, count = slot_of(step, part), blocks_of(step, part)[1]
@@ -573,15 +568,13 @@
             if step == 0 and index == 0:
                 returned[me] = total[0, spot]
             else:
-                begin(
-                    remote(
-                        total.at[slot, spot],
-                        returned.at[me],
-                        far_send.at[step, index],
-                        far_recv.at[me],
-                        sp=block,
-                    )
-                )
+                remote(
+                    total.at[slot, spot],
+                    returned.at[me],
+                    far_send.at[0],
+                    far_recv.at[me],
+                    sp=block,
+                ).start()
 
     stage_select(0)
 
@@ -730,7 +723,7 @@
     for step in range(1, sp_count):
         source = lax.rem(me + step, sp_count)
         remote(
-            total.at[0, 0], returned.at[source], far_send.at[0, 0], far_recv.at[source], sp=source
+            total.at[0, 0], returned.at[source], far_send.at[0], far_recv.at[source], sp=source
         ).wait_recv()
     routed_sum = jnp.dot(
         picks_t[...],
@@ -858,6 +851,17 @@
             @pl.when(goes_on(step))
             def _():
                 chain_on(which, step).wait_send()
+
+    def drain(ref, sem):
+        remote(ref, ref, sem, parts_recv.at[0], tp=partner).wait_send()
+
+    drain(both.at[0, pl.ds(0, sp_count - 1)], twin_send.at[0])
+    drain(near_out, cross_send.at[0])
+    drain(cross_out, cross_send.at[1])
+    drain(both.at[0, pl.ds(0, (layers - 2) * (chips - 1))], along_send.at[0])
+    drain(both.at[0, pl.ds(0, sp_count // 2)], pair_send.at[0])
+    drain(both.at[0, pl.ds(0, sp_count * (chips - 1) // tp_count)], side_send.at[0])
+    drain(returned.at[pl.ds(0, sp_count - 1)], far_send.at[0])
 
 
 def fused(
@@ -936,12 +940,12 @@
             dma((2, 2, chips - 1)),
             dma((2, 2, chips - 1)),
         ]
-        + [dma((2, layers, across - 1, chips))] * 2
-        + [dma((2, layers - 2, across, chips - 1))] * 2
-        + [dma((2, layers, across, chips))] * 2
-        + [dma((slots, chips))] * 2
-        + [dma((slots, chips - 1))] * 2
-        + [dma((layers, across)), dma((sp_count,))]
+        + [dma((2,)), dma((2, layers, across - 1, chips))]
+        + [dma((1,)), dma((2, layers - 2, across, chips - 1))]
+        + [dma((1,)), dma((2, layers, across, chips))]
+        + [dma((1,)), dma((slots, chips))]
+        + [dma((1,)), dma((slots, chips - 1))]
+        + [dma((1,)), dma((sp_count,))]
         + [dma((2, chips))] * 2
         + [dma((2, tp_count - 1))] * 2
         + [dma((sp_count,))] * 2

time: 114 us -> 112 us (0.982)
  Pallas kernels: 113 us -> 111 us
    pallas_call x1, Pallas kernels: 108 us -> 106 us  [fused(): pl.pallas_call(functools.partial(fused_kernel, sp_count, tp_count), out_s...]
where the time goes in v4:
time: 112 us; the launch traced here: 111 us
  Pallas kernels  111 us (99%)
    pallas_call x1, Pallas kernels, fused(): pl.pallas_call(functools.partial(fused_kernel, sp_count, tp_count), out_s...  106 us
    pallas_call x1, Pallas kernels, emit(): pl.pallas_call(emit_kernel, out_shape=tuple((jax.ShapeDtypeStruct(item.sh...  4.76 us

profile of v4, /device:TPU:23, one launch (start us, length us, event | category | flops | bytes accessed | tf_op | source)
XLA Modules:
  0.0 111.4 jit_solution(8851471660556734923)
XLA Ops:
  0.6 105.9 %fused.1 = (bf16[256,512]{1,0:T(8,128)(2,1)S(1)}, bf16[256,128]{1,0:T(8,128)(2,1)S(1)}, bf16[256,128]{1,0:T(8,128)(2,1)S(1)}, f32[256,128]{1,0:T(8,128)S(1)}, f3...) custom-call(s32[2,256]{1,0:T(2,128)} %bitcast.2, f32[2,256]{1,0:T(2,128)} %bitcast.3, ...), custom_call_target="tpu_custom_call" | custom-call | tf_op jit(solution)/shard_map/fused/pallas_call | solution.py:886
  106.5 4.8 %emit.1 = (bf16[256,512]{1,0:T(8,128)(2,1)}, bf16[256,128]{1,0:T(8,128)(2,1)}, bf16[256,128]{1,0:T(8,128)(2,1)}, f32[256,128]{1,0:T(8,128)}, f32[1,2048,512]{2,1...) custom-call(bf16[256,512]{1,0:T(8,128)(2,1)S(1)} %get-tuple-element.14.refs_0_, ...), custom_call_target="tpu_custom_call" | custom-call | tf_op jit(solution)/shard_map/emit/pallas_call | solution.py:973

commit v5 on v4

--- a/solution.py
+++ b/solution.py
@@ -216,13 +216,13 @@
         return remote(
             meta_ref,
             metas.at[layer],
-            meta_send.at[step],
+            meta_send.at[0],
             meta_recv.at[layer],
             sp=lax.rem(me + step * across, sp_count),
         )
 
     for step in range(1, layers):
-        begin(give_meta(step))
+        give_meta(step).start()
 
     def own_chain(which, up):
         to = me + across if up else me + sp_count - across
@@ -587,7 +587,7 @@
         return remote(
             stat_out.at[phase],
             stat_in.at[phase, hop],
-            stat_send.at[phase, hop - 1],
+            stat_send.at[0],
             stat_recv.at[phase, hop - 1],
             tp=lax.rem(lane + hop, tp_count),
         )
@@ -602,7 +602,7 @@
                 stat_out[phase, row : row + 1] = jnp.sum(spread, axis=0, keepdims=True)
                 row += 1
         for hop in range(1, tp_count):
-            begin(stat(phase, hop))
+            stat(phase, hop).start()
 
     def shared(phase):
         value = stat_out[phase]
@@ -647,10 +647,10 @@
         stage_forward(step)
     stage_cross(0)
     stage_expert(0)
+    if layers > 2:
+        stage_cross(1)
     stage_pair(0)
     for step in range(2, layers):
-        if step == 2:
-            stage_cross(1)
         if step < last:
             stage_select(step)
         else:
@@ -671,8 +671,9 @@
         stage_expert(step - 1)
         if step == last:
             stage_extra()
+        stage_pair(step - 1)
+        if step == last:
             stage_return(step - 2)
-        stage_pair(step - 1)
     if split_last:
         stage_expert(last, 0)
         stage_pair(last, 0)
@@ -738,7 +739,7 @@
         return remote(
             full.at[:, columns(lane)],
             full.at[:, columns(lane)],
-            full_send.at[0, hop],
+            full_send.at[0],
             full_recv.at[0, hop],
             tp=lax.rem(lane + 2 * hop, tp_count),
         )
@@ -748,17 +749,17 @@
         return remote(
             full.at[:, columns(column)],
             full.at[:, columns(column)],
-            full_send.at[1, hop],
+            full_send.at[0],
             full_recv.at[1, hop],
             tp=partner,
         )
 
     for hop in range(1, chips):
-        begin(spread_full(hop))
-    begin(hand_over(0))
+        spread_full(hop).start()
+    hand_over(0).start()
     for hop in range(1, chips):
         spread_full(hop).wait_recv()
-        begin(hand_over(hop))
+        hand_over(hop).start()
     for hop in range(chips):
         hand_over(hop).wait_recv()
 
@@ -774,13 +775,13 @@
         return remote(
             parts_out.at[to],
             parts_in.at[step],
-            parts_send.at[step],
+            parts_send.at[0],
             parts_recv.at[step],
             sp=to,
         )
 
     for step in range(1, sp_count):
-        begin(give_parts(step))
+        give_parts(step).start()
 
     grad_mixed = jnp.dot(full[...], proj_ref[...], preferred_element_type=f32)
     grad_normed = grad_mixed * norm_sigmoid * (1.0 + normed * (1.0 - norm_sigmoid))
@@ -862,6 +863,10 @@
     drain(both.at[0, pl.ds(0, sp_count // 2)], pair_send.at[0])
     drain(both.at[0, pl.ds(0, sp_count * (chips - 1) // tp_count)], side_send.at[0])
     drain(returned.at[pl.ds(0, sp_count - 1)], far_send.at[0])
+    drain(parts_in.at[pl.ds(0, sp_count - 1)], parts_send.at[0])
+    drain(full.at[:, pl.ds(0, (tp_count - 1) * width)], full_send.at[0])
+    drain(stat_in.at[:, pl.ds(0, tp_count - 1)], stat_send.at[0])
+    drain(metas.at[pl.ds(0, layers - 1)], meta_send.at[0])
 
 
 def fused(
@@ -933,7 +938,7 @@
             vmem((rim, channels), f32),
             vmem((tok_count + rim, channels), f32),
             dma((10,)),
-            dma((layers,)),
+            dma((1,)),
             dma((layers,)),
             dma((2, layers, 2)),
             dma((2, layers)),
@@ -946,9 +951,9 @@
         + [dma((1,)), dma((slots, chips))]
         + [dma((1,)), dma((slots, chips - 1))]
         + [dma((1,)), dma((sp_count,))]
-        + [dma((2, chips))] * 2
-        + [dma((2, tp_count - 1))] * 2
-        + [dma((sp_count,))] * 2
+        + [dma((1,)), dma((2, chips))]
+        + [dma((1,)), dma((2, tp_count - 1))]
+        + [dma((1,)), dma((sp_count,))]
         + [dma((1,))] * 2,
         compiler_params=pltpu.CompilerParams(
             collective_id=0, has_side_effects=True, vmem_limit_bytes=47 * 1024 * 1024

time: 112 us -> 111 us (level)
  no operation moved by 1% of the time
where the time goes in v5:
time: 111 us
  Pallas kernels  110 us (99%)
    pallas_call x1, Pallas kernels, fused(): pl.pallas_call(functools.partial(fused_kernel, sp_count, tp_count), out_s...  105 us
    pallas_call x1, Pallas kernels, emit(): pl.pallas_call(emit_kernel, out_shape=tuple((jax.ShapeDtypeStruct(item.sh...  4.76 us

profile of v5, /device:TPU:23, one launch (start us, length us, event | category | flops | bytes accessed | tf_op | source)
XLA Modules:
  0.0 110.6 jit_solution(14594176371389157455)
XLA Ops:
  0.6 105.1 %fused.1 = (bf16[256,512]{1,0:T(8,128)(2,1)S(1)}, bf16[256,128]{1,0:T(8,128)(2,1)S(1)}, bf16[256,128]{1,0:T(8,128)(2,1)S(1)}, f32[256,128]{1,0:T(8,128)S(1)}, f3...) custom-call(s32[2,256]{1,0:T(2,128)} %bitcast.2, f32[2,256]{1,0:T(2,128)} %bitcast.3, ...), custom_call_target="tpu_custom_call" | custom-call | tf_op jit(solution)/shard_map/fused/pallas_call | solution.py:891
  105.7 4.8 %emit.1 = (bf16[256,512]{1,0:T(8,128)(2,1)}, bf16[256,128]{1,0:T(8,128)(2,1)}, bf16[256,128]{1,0:T(8,128)(2,1)}, f32[256,128]{1,0:T(8,128)}, f32[1,2048,512]{2,1...) custom-call(bf16[256,512]{1,0:T(8,128)(2,1)S(1)} %get-tuple-element.14.refs_0_, ...), custom_call_target="tpu_custom_call" | custom-call | tf_op jit(solution)/shard_map/emit/pallas_call | solution.py:978
